TPU v7x, 32 devices: a whole 2x2x4 slice. The times are simulated.
32 devices in a mesh: ep: 8 (over z, x), tp: 4 (over y, core).
Axes of the slice: x: 2, y: 2, z: 4, core: 2. Of those that a mesh axis runs over, the one named last changes fastest.
Arguments:
- tokens: bfloat16 [192, 4096], P('ep'), may hold values from -6 to 6
- delta_state: float32 [192, 16, 128, 128], P('ep', 'tp'), may hold values from -0.625 to 0.625
- attn_gain: float32 [4096], replicated, may hold values from 0.1 to 1.9
- query_weight: bfloat16 [4096, 2048], P('ep', 'tp'), may hold values from -0.09375 to 0.09375
- key_weight: bfloat16 [4096, 2048], P('ep', 'tp'), may hold values from -0.09375 to 0.09375
- value_weight: bfloat16 [4096, 2048], P('ep', 'tp'), may hold values from -0.09375 to 0.09375
- decay_weight: bfloat16 [4096, 16], replicated, may hold values from -0.09375 to 0.09375
- beta_weight: bfloat16 [4096, 16], replicated, may hold values from -0.09375 to 0.09375
- decay_rate: float32 [16], P('tp'), may hold values from 0.05 to 3
- head_gain: float32 [128], replicated, may hold values from 0.1 to 1.9
- output_weight: bfloat16 [2048, 4096], P('tp'), may hold values from -0.125 to 0.125
- ffn_gain: float32 [4096], replicated, may hold values from 0.1 to 1.9
- expert_ids: int32 [192, 2], P('ep'), may hold values from 0 to 7, all different within a row; in each aligned block of 24 rows (0 to 23, 24 to 47, ...) at most 12 rows name the same one
- group_prob: float32 [192], P('ep'), may hold values from 0.3 to 1
- expert_logit: float32 [192, 2], P('ep'), may hold values from -8 to 8
- expert_gate: bfloat16 [8, 4096, 1024], P('ep', None, 'tp'), may hold values from -0.09375 to 0.09375
- expert_up: bfloat16 [8, 4096, 1024], P('ep', None, 'tp'), may hold values from -0.09375 to 0.09375
- expert_down: bfloat16 [8, 1024, 4096], P('ep', 'tp'), may hold values from -0.1875 to 0.1875
- dense_gate: bfloat16 [4096, 4096], P('tp', 'ep'), may hold values from -0.09375 to 0.09375
- dense_up: bfloat16 [4096, 4096], P('tp', 'ep'), may hold values from -0.09375 to 0.09375
- dense_down: bfloat16 [4096, 4096], P('ep', 'tp'), may hold values from -0.09375 to 0.09375
- dense_mix: float32 [4096], P('tp'), may hold values from -3 to 3
Outputs:
- mixed_out: bfloat16 [192, 4096], P('ep', 'tp')
- new_state: float32 [192, 16, 128, 128], P('ep', 'tp')
Inputs may be any that keep to these rules, and one draw needn't show every extreme that they name: `expert_ids`: each row names 2 different experts. Among the rows of one device (aligned blocks of 24 rows) no expert is named by more than 12 rows, and in every draw some expert reaches 12 in some block.
All inputs are finite; a program needn't handle non-finite values.
Results may differ from a plain program's by a relative error of at most 0.02.
Values may be sent and summed in bfloat16 or wider, within the bound.
A program may use at most 64 MiB of HBM per device.

v0:
```python
import functools
import math

import jax
import jax.numpy as jnp
from jax import lax
from jax.experimental import pallas as pl
from jax.experimental.pallas import tpu as pltpu
from jax.sharding import PartitionSpec as P

EPS = 1e-06
BF = jnp.bfloat16
F32 = jnp.float32
MESH = pl.DeviceIdType.MESH


def dot(left, right):
    return jnp.dot(left, right, preferred_element_type=F32)


def dot_t(left, right):
    return lax.dot_general(left, right, (((1,), (1,)), ((), ())), preferred_element_type=F32)


def silu(values):
    return values / (1.0 + jnp.exp(-values))


class BlockOf:
    def __init__(self, ref, block):
        self.ref, self.block = ref, block

    @property
    def at(self):
        return self

    def __getitem__(self, index):
        return self.ref.at[index, self.block]


def kernel(dims, *refs):
    n_ep, n_tp, rows, width, heads, members, cap, n_in, n_weights = dims
    inputs, refs = refs[:n_in], refs[n_in:]
    (tokens, attn_gain, decay_rate, head_gain, ffn_gain, ids, group_prob, logit, mix) = inputs[:9]
    hbm = inputs[9:]
    out, key_out, corr_out, decay_out = refs[:4]
    held = refs[4 : 4 + n_weights]
    refs = refs[4 + n_weights :]
    state, w_decay, w_beta, w_q, w_k, w_v, w_o, w_dg, w_du, w_eg, w_eu, w_ed, w_dd = held
    (
        n_send, n_recv, q_send, q_recv, c_send, c_recv, kq, recall, head_out,
        a_send, a_recv, s_recv, middle_ref, x_all, g_all, d_send, d_recv, h_all,
        e_send, e_recv, f_send, f_recv, place_ref, dense_ref, load_sem, ep_send, ep_recv, tp_send, tp_recv,
    ) = refs
    me = lax.axis_index("ep")
    my = lax.axis_index("tp")
    chunk = width // n_tp
    depth = width // n_ep
    batch = n_ep * rows
    local = heads * 128
    groups = n_ep // members
    group_slots = members * cap
    group_tokens = members * rows
    slots = groups * group_slots
    my_group = lax.div(me, members)
    my_member = lax.rem(me, members)

    def members_of(offset):
        first = lax.rem(my_group + offset + groups, groups) * members
        start = 1 if offset == 0 else 0
        return [first + lax.rem(my_member + m, members) for m in range(start, members)]

    loads = [
        pltpu.make_async_copy(src, dst, load_sem.at[i])
        for i, (src, dst) in enumerate(zip(hbm, held))
    ]
    state_i, decay_i, beta_i, q_i, k_i, v_i, o_i, dg_i, du_i, eg_i, eu_i, ed_i, dd_i = range(13)
    order = (decay_i, beta_i, q_i, k_i, v_i, state_i, o_i, dg_i, du_i, eg_i, eu_i, ed_i, dd_i)

    ep_peers = [p for offset in range(groups) for p in members_of(offset)]
    tp_peers = [lax.rem(my + d, n_tp) for d in range(1, n_tp)]
    barrier = pltpu.get_barrier_semaphore()
    for p in ep_peers:
        pl.semaphore_signal(barrier, inc=1, device_id=(p, my), device_id_type=MESH)
    for p in tp_peers:
        pl.semaphore_signal(barrier, inc=1, device_id=(me, p), device_id_type=MESH)
    for i in order:
        loads[i].start()

    def ep_copy(phase, src, dst, peer, source):
        return pltpu.make_async_remote_copy(
            src_ref=src, dst_ref=dst,
            send_sem=ep_send.at[phase, peer], recv_sem=ep_recv.at[phase, source],
            device_id=(peer, my), device_id_type=MESH,
        )

    def tp_copy(phase, src, dst, peer, source):
        return pltpu.make_async_remote_copy(
            src_ref=src, dst_ref=dst,
            send_sem=tp_send.at[phase, peer], recv_sem=tp_recv.at[phase, source],
            device_id=(me, peer), device_id_type=MESH,
        )

    def exchange(copy, phase, peers, mine, src_of, dst):
        for p in peers:
            copy(phase, src_of(p), dst.at[mine], p, mine).start()

        def arrived():
            for p in peers:
                done = copy(phase, src_of(p), dst.at[p], p, p)
                done.wait_recv()
                done.wait_send()

        return arrived

    x = tokens[...].astype(F32)
    mean_sq = jnp.mean(x * x, axis=-1, keepdims=True)
    normed = (x * lax.rsqrt(mean_sq + EPS) * attn_gain[...]).astype(BF)
    for p in range(n_ep):
        n_send[p] = normed[:, p * depth : (p + 1) * depth]
    pl.semaphore_wait(barrier, n_ep + n_tp - 2)
    wait_n = exchange(ep_copy, 0, ep_peers, me, lambda p: n_send.at[p], n_recv)
    n_recv[me] = n_send[me]

    logit_exp = jnp.exp(logit[...])
    route = group_prob[...] * logit_exp / jnp.sum(logit_exp, axis=0, keepdims=True)
    names = ids[...]
    eye = lax.broadcasted_iota(jnp.int32, (rows, rows), 0) == lax.broadcasted_iota(
        jnp.int32, (rows, rows), 1
    )
    for p in range(n_ep):
        flat = jnp.sum(jnp.where(names == p, route, 0.0), axis=0, keepdims=True)
        coef = jnp.sum(jnp.where(eye, flat, 0.0), axis=1, keepdims=True)
        c_send[p] = jnp.broadcast_to(coef, (rows, 128))
    loads[decay_i].wait()
    loads[beta_i].wait()
    decay_pre = dot_t(normed, w_decay[...])
    beta_pre = dot_t(normed, w_beta[...])
    lane = lax.broadcasted_iota(jnp.int32, decay_pre.shape, 1)
    decays, betas = [], []
    for h in range(heads):
        mine = lane == my * heads + h
        d = jnp.sum(jnp.where(mine, decay_pre, 0.0), axis=1, keepdims=True)
        b = jnp.sum(jnp.where(mine, beta_pre, 0.0), axis=1, keepdims=True)
        soft = jnp.maximum(d, 0.0) + jnp.log1p(jnp.exp(-jnp.abs(d)))
        decays.append(jnp.exp(-decay_rate[:, h : h + 1] * soft))
        betas.append(1.0 / (1.0 + jnp.exp(-b)))
    for i in (q_i, k_i, v_i):
        loads[i].wait()

    wait_n()
    spread = n_recv[...].astype(F32).reshape(batch, depth).astype(BF)
    wait_heads = []
    for j, w in enumerate((w_k, w_q, w_v)):
        part = dot(spread, w[...]).reshape(n_ep, rows, local)
        q_send[j] = part.astype(BF)
        wait_heads.append(
            exchange(ep_copy, 1 + j, ep_peers, me, lambda p, j=j: q_send.at[j, p], q_recv.at[j])
        )
        q_recv[j, me] = q_send[j, me]

    def summed(j):
        wait_heads[j]()
        total = q_recv[j, 0].astype(F32)
        for p in range(1, n_ep):
            total = total + q_recv[j, p].astype(F32)
        return total.astype(BF).astype(F32)

    k_rows = summed(0)
    q_rows = summed(1)
    loads[state_i].wait()

    def head_of(values, h):
        return values[:, h * 128 : (h + 1) * 128]

    def unit(values):
        return values * lax.rsqrt(jnp.sum(values * values, axis=-1, keepdims=True) + EPS)

    units = []
    for h in range(heads):
        q_unit = unit(head_of(q_rows, h)) * 128 ** (-0.5)
        k_unit = unit(head_of(k_rows, h))
        units.append((q_unit, k_unit))
        kq[:, h, :] = k_unit
        kq[:, heads + h, :] = q_unit

    def one_row(b, _):
        columns = kq[b].T
        for h in range(heads):
            block = state[b, h]
            recall[h, pl.ds(b, 1), :] = jnp.sum(columns[:, h : h + 1] * block, axis=0, keepdims=True)
            recall[heads + h, pl.ds(b, 1), :] = jnp.sum(
                columns[:, heads + h : heads + h + 1] * block, axis=0, keepdims=True
            )
        return 0

    lax.fori_loop(0, rows, one_row, 0)
    v_rows = summed(2)
    wait_c = exchange(ep_copy, 4, ep_peers, me, lambda p: c_send.at[p], c_recv)
    c_recv[me] = c_send[me]
    for h in range(heads):
        q_unit, k_unit = units[h]
        decay, beta = decays[h], betas[h]
        corr = beta * (head_of(v_rows, h) - decay * recall[h])
        read = decay * recall[heads + h] + jnp.sum(q_unit * k_unit, axis=-1, keepdims=True) * corr
        read = read * lax.rsqrt(jnp.mean(read * read, axis=-1, keepdims=True) + EPS) * head_gain[...]
        head_out[:, h * 128 : (h + 1) * 128] = read.astype(BF)
        key_out[:, h, :] = k_unit
        corr_out[:, h, :] = corr
        decay_out[:, h, :] = jnp.broadcast_to(decay, (rows, 128))

    loads[o_i].wait()
    ho = head_out[...]
    for c in range(n_tp):
        a_send[c] = dot(ho, w_o[:, c * chunk : (c + 1) * chunk]).astype(BF)
    wait_a = exchange(tp_copy, 0, tp_peers, my, lambda p: a_send.at[p], a_recv)
    a_recv[my] = a_send[my]
    own = pl.ds(pl.multiple_of(my * chunk, 128), chunk)
    middle = tokens[:, own].astype(F32)
    wait_a()
    for p in range(n_tp):
        middle = middle + a_recv[p].astype(F32)
    middle_ref[...] = middle
    s_recv[my] = jnp.broadcast_to(jnp.sum(middle * middle, axis=-1, keepdims=True), (rows, 128))
    wait_s = exchange(tp_copy, 1, tp_peers, my, lambda p: s_recv.at[my], s_recv)
    wait_c()
    tri = (
        lax.broadcasted_iota(jnp.int32, (group_tokens, group_tokens), 0)
        >= lax.broadcasted_iota(jnp.int32, (group_tokens, group_tokens), 1)
    ).astype(F32).astype(BF)
    slot = lax.broadcasted_iota(jnp.int32, (group_tokens, group_slots), 1).astype(F32)
    for g in range(groups):
        coef = c_recv[g * members : (g + 1) * members].reshape(group_tokens, 128)[:, :1]
        named = coef > 0.0
        flags = jnp.broadcast_to(jnp.where(named, 1.0, 0.0), (group_tokens, 128)).astype(BF)
        rank = dot(tri, flags)[:, :1] - 1.0
        place_ref[g] = jnp.where((rank == slot) & named, 1.0, 0.0).astype(BF)
    wait_s()
    total = s_recv[0]
    for p in range(1, n_tp):
        total = total + s_recv[p]
    scale = lax.rsqrt(total[:, :1] / width + EPS)
    x_all[me] = (middle * scale * ffn_gain[:, own]).astype(BF)
    for p in ep_peers:
        ep_copy(5, x_all.at[me], x_all.at[me], p, me).start()
    wait_g = []
    for offset in range(groups):
        g = lax.rem(my_group - offset + groups, groups)
        for p in members_of(-offset):
            ep_copy(5, x_all.at[me], x_all.at[p], p, p).wait_recv()
        block = x_all[pl.ds(g * members, members)].astype(F32)
        g_all[my, g] = lax.dot_general(
            place_ref[g], block.reshape(group_tokens, chunk).astype(BF),
            (((0,), (0,)), ((), ())), preferred_element_type=F32,
        ).astype(BF)
        wait_g.append(
            exchange(
                tp_copy, 4 + offset, tp_peers, my, lambda p, g=g: g_all.at[my, g],
                BlockOf(g_all, g),
            )
        )
    for p in ep_peers:
        ep_copy(5, x_all.at[me], x_all.at[me], p, me).wait_send()
    for i in (dg_i, du_i, eg_i, eu_i, ed_i, dd_i):
        loads[i].wait()
    xs = x_all[...].astype(F32).reshape(batch, chunk).astype(BF)
    hidden = w_dg.shape[1]
    part_rows = batch // n_tp
    for j, w in enumerate((w_dg, w_du)):
        part = dot(xs, w[...]).reshape(n_tp, part_rows, hidden)
        d_send[:, :, j * hidden : (j + 1) * hidden] = part.astype(BF)
    wait_d = exchange(tp_copy, 2, tp_peers, my, lambda p: d_send.at[p], d_recv)
    d_recv[my] = d_send[my]

    for wait in wait_g:
        wait()
    gate = jnp.zeros((slots, w_eg.shape[2]), F32)
    up = jnp.zeros((slots, w_eg.shape[2]), F32)
    for c in range(n_tp):
        routed = g_all[c].astype(F32).reshape(slots, chunk).astype(BF)
        gate = gate + dot(routed, w_eg[0, c * chunk : (c + 1) * chunk, :])
        up = up + dot(routed, w_eu[0, c * chunk : (c + 1) * chunk, :])
    expert_hidden = (silu(gate) * up).astype(BF)
    for c in range(n_tp):
        part = dot(expert_hidden, w_ed[0, :, c * chunk : (c + 1) * chunk])
        e_send[c] = part.reshape(groups, group_slots, chunk).astype(BF)
    e_recv[my] = e_send[my]
    returns = list(range(1, groups)) + [0]
    group_at = [lax.rem(my_group + offset, groups) for offset in range(groups)]

    def send_e(offset):
        g = group_at[offset]
        return exchange(
            tp_copy, 4 + groups + offset, tp_peers, my, lambda p: e_send.at[p, g],
            BlockOf(e_recv, g),
        )

    wait_e = {returns[0]: send_e(returns[0])}
    wait_d()
    pre = d_recv[0].astype(F32)
    for p in range(1, n_tp):
        pre = pre + d_recv[p].astype(F32)
    h_all[my] = (silu(pre[:, :hidden]) * pre[:, hidden:]).astype(BF)
    wait_h = exchange(tp_copy, 3, tp_peers, my, lambda p: h_all.at[my], h_all)
    for offset in returns[1:]:
        wait_e[offset] = send_e(offset)
    wait_h()
    dense_hidden = h_all[...].astype(F32).reshape(batch, hidden).astype(BF)
    dense = dot(dense_hidden, w_dd[...]) * (1.0 / (1.0 + jnp.exp(-mix[...])))
    dense_ref[...] = dense.reshape(n_ep, rows, chunk)
    for offset in returns:
        g = group_at[offset]
        here = pl.ds(g * members, members)
        wait_e[offset]()
        result = e_recv[0, g].astype(F32)
        for p in range(1, n_tp):
            result = result + e_recv[p, g].astype(F32)
        coef = c_recv[here].reshape(group_tokens, 128)[:, :1]
        mixed = coef * dot(place_ref[g], result.astype(BF))
        combined = dense_ref[here] + mixed.reshape(members, rows, chunk)
        f_send[here] = combined.astype(BF)
        for p in members_of(offset):
            ep_copy(6, f_send.at[p], f_recv.at[me], p, me).start()
    final = middle_ref[...] + f_send[me].astype(F32)
    f_recv[me] = jnp.zeros((rows, chunk), BF)
    for p in ep_peers:
        done = ep_copy(6, f_send.at[p], f_recv.at[p], p, p)
        done.wait_recv()
        done.wait_send()
    for p in range(n_ep):
        final = final + f_recv[p].astype(F32)
    out[...] = final.astype(BF)


def per_device(
    tokens, delta_state, attn_gain, query_weight, key_weight, value_weight, decay_weight,
    beta_weight, decay_rate, head_gain, output_weight, ffn_gain, expert_ids, group_prob,
    expert_logit, expert_gate, expert_up, expert_down, dense_gate, dense_up, dense_down, dense_mix,
):
    n_ep = lax.axis_size("ep")
    n_tp = lax.axis_size("tp")
    rows, width = tokens.shape
    heads = delta_state.shape[1]
    local = heads * 128
    topk = expert_ids.shape[1]
    cap = max(2, 2 * rows * topk // n_ep)
    members = 8 // math.gcd(cap, 8)
    if n_ep % members:
        members = n_ep
    groups = n_ep // members
    group_slots = members * cap
    chunk = width // n_tp
    depth = width // n_ep
    batch = n_ep * rows
    hidden = dense_gate.shape[1]
    small = (
        tokens, attn_gain[None, :], decay_rate[None, :], head_gain[None, :], ffn_gain[None, :],
        expert_ids.T, group_prob[None, :], expert_logit.T, dense_mix[None, :],
    )
    weights = (
        delta_state, decay_weight.T, beta_weight.T, query_weight, key_weight, value_weight,
        output_weight, dense_gate, dense_up, expert_gate, expert_up, expert_down, dense_down,
    )
    dims = (n_ep, n_tp, rows, width, heads, members, cap, len(small) + len(weights), len(weights))
    vmem = pl.BlockSpec(memory_space=pltpu.VMEM)
    kq_rows = -(-2 * heads // 8) * 8
    scratch = [pltpu.VMEM(w.shape, w.dtype) for w in weights]
    scratch += [
        pltpu.VMEM(shape, dtype)
        for shape, dtype in (
            ((n_ep, rows, depth), BF), ((n_ep, rows, depth), BF),
            ((3, n_ep, rows, local), BF), ((3, n_ep, rows, local), BF),
            ((n_ep, rows, 128), F32), ((n_ep, rows, 128), F32),
            ((rows, kq_rows, 128), F32), ((2 * heads, rows, 128), F32), ((rows, local), BF),
            ((n_tp, rows, chunk), BF), ((n_tp, rows, chunk), BF), ((n_tp, rows, 128), F32),
            ((rows, chunk), F32), ((n_ep, rows, chunk), BF), ((n_tp, groups, group_slots, chunk), BF),
            ((n_tp, batch // n_tp, 2 * hidden), BF), ((n_tp, batch // n_tp, 2 * hidden), BF),
            ((n_tp, batch // n_tp, hidden), BF),
            ((n_tp, groups, group_slots, chunk), BF), ((n_tp, groups, group_slots, chunk), BF),
            ((n_ep, rows, chunk), BF), ((n_ep, rows, chunk), BF),
            ((groups, members * rows, group_slots), BF), ((n_ep, rows, chunk), F32),
        )
    ]
    scratch += [
        pltpu.SemaphoreType.DMA((len(weights),)),
        pltpu.SemaphoreType.DMA((7, n_ep)), pltpu.SemaphoreType.DMA((7, n_ep)),
        pltpu.SemaphoreType.DMA((4 + 2 * groups, n_tp)), pltpu.SemaphoreType.DMA((4 + 2 * groups, n_tp)),
    ]
    per_head = jax.ShapeDtypeStruct((rows, heads, 128), F32)
    mixed_out, key, corr, decay = pl.pallas_call(
        functools.partial(kernel, dims),
        out_shape=(jax.ShapeDtypeStruct((rows, chunk), BF), per_head, per_head, per_head),
        in_specs=[vmem] * len(small) + [pl.BlockSpec(memory_space=pl.ANY)] * len(weights),
        out_specs=(vmem,) * 4,
        scratch_shapes=scratch,
        compiler_params=pltpu.CompilerParams(
            collective_id=0, has_side_effects=True, vmem_limit_bytes=62 * 1024 * 1024
        ),
    )(*small, *weights)
    new_state = decay[:, :, None, :] * delta_state + key[..., :, None] * corr[..., None, :]
    return mixed_out, new_state


def solution(mesh):
    return jax.shard_map(
        per_device,
        mesh=mesh,
        in_specs=(
            P("ep", None), P("ep", "tp", None, None), P(), P("ep", "tp"), P("ep", "tp"),
            P("ep", "tp"), P(), P(), P("tp"), P(), P("tp", None), P(), P("ep", None), P("ep"),
            P("ep", None), P("ep", None, "tp"), P("ep", None, "tp"), P("ep", "tp", None),
            P("tp", "ep"), P("tp", "ep"), P("ep", "tp"), P("tp"),
        ),
        out_specs=(P("ep", "tp"), P("ep", "tp", None, None)),
        check_vma=False,
    )
```

profile of v0, /device:TPU:0, one launch (start us, length us, event | category | flops | bytes accessed | tf_op | source)
XLA Modules:
  0.0 87.0 jit_solution(17993009548093498984)
XLA Ops:
  0.6 78.3 %shard_map.221 = (bf16[24,1024]{1,0:T(8,128)(2,1)}, f32[24,4,128]{2,1,0:T(4,128)}, f32[24,4,128]{2,1,0:T(4,128)}, f32[24,4,128]{2,1,0:T(4,128)}) custom-call(bf16[24,4096]{1,0:T(8,128)(2,1)} %refs_0_.1, f32[1,4096]{1,0:T(1,128)} %bitcast.12, f32[1,4]{1,0:T(1,128)} %bitcast.17, f32[1,128]{1,0:T(1,128)} %bitcast.18, f32[1,4096]{1,0:T(1,128)} %bitcast.13, ...), custom_call_target="tpu_custom_call" | custom-call | tf_op jit(solution)/shard_map/pallas_call | solution.py:390
  79.0 0.0 copy-start
  79.0 7.4 %multiply_add_fusion = f32[24,4,128,128]{3,2,1,0:T(8,128)} fusion(f32[24,4,128,128]{3,2,1,0:T(8,128)} %refs_9_.1, f32[24,4,128]{2,1,0:T(4,128)} %get-tuple-element.9, f32[24,4,128]{2,1,0:T(4,128)} %get-tuple-element.8, f32[24,4,128]{2,1,0:T(4,128)} %get-tuple-element.7), kind=kLoop, calls=%fused_computation | loop fusion | flops 4718592 | bytes 12730368 | tf_op jit(solution)/shard_map/add | solution.py:400
  86.4 0.0 copy-done
  86.4 0.6 copy.25
Async XLA Ops:
  79.0 7.4 %copy-start = (bf16[24,1024]{1,0:T(8,128)(2,1)S(1)}, bf16[24,1024]{1,0:T(8,128)(2,1)}, u32[]{:S(2)}) copy-start(bf16[24,1024]{1,0:T(8,128)(2,1)} %get-tuple-element.12) | copy-start | bytes 147460
where the time goes:
time: 87.2 us; the launch traced here: 87 us
  Pallas kernels  78.3 us (90%)
  other arithmetic  7.37 us (8%)
    pallas_call x1, Pallas kernels, per_device(): pl.pallas_call(functools.partial(kernel, dims), out_shape=(jax.ShapeDtype...  78.3 us
    add x1, other arithmetic, per_device(): decay[:, :, None, :] * delta_state + key[..., :, None] * corr[..., None, :]  7.37 us

commit v1 on v0

--- a/solution.py
+++ b/solution.py
@@ -43,13 +43,13 @@
     inputs, refs = refs[:n_in], refs[n_in:]
     (tokens, attn_gain, decay_rate, head_gain, ffn_gain, ids, group_prob, logit, mix) = inputs[:9]
     hbm = inputs[9:]
-    out, key_out, corr_out, decay_out = refs[:4]
-    held = refs[4 : 4 + n_weights]
-    refs = refs[4 + n_weights :]
+    out, state = refs[:2]
+    held = (state,) + refs[2 : 1 + n_weights]
+    refs = refs[1 + n_weights :]
     state, w_decay, w_beta, w_q, w_k, w_v, w_o, w_dg, w_du, w_eg, w_eu, w_ed, w_dd = held
     (
-        n_send, n_recv, q_send, q_recv, c_send, c_recv, kq, recall, head_out,
-        a_send, a_recv, s_recv, middle_ref, x_all, g_all, d_send, d_recv, h_all,
+        n_send, n_recv, q_send, q_recv, c_send, c_rows, c_recv, kq, recall, corr_ref, decay_ref,
+        head_out, a_send, a_recv, s_recv, scale_rows, scale_ref, middle_ref, x_all, g_all, d_send, d_recv, h_all,
         e_send, e_recv, f_send, f_recv, place_ref, dense_ref, load_sem, ep_send, ep_recv, tp_send, tp_recv,
     ) = refs
     me = lax.axis_index("ep")
@@ -128,10 +128,16 @@
     eye = lax.broadcasted_iota(jnp.int32, (rows, rows), 0) == lax.broadcasted_iota(
         jnp.int32, (rows, rows), 1
     )
+    c_send[...] = jnp.zeros_like(c_send)
     for p in range(n_ep):
         flat = jnp.sum(jnp.where(names == p, route, 0.0), axis=0, keepdims=True)
-        coef = jnp.sum(jnp.where(eye, flat, 0.0), axis=1, keepdims=True)
-        c_send[p] = jnp.broadcast_to(coef, (rows, 128))
+        c_send[p, :, :rows] = jnp.broadcast_to(flat, (8, rows))
+    wait_c = exchange(ep_copy, 4, ep_peers, me, lambda p: c_send.at[p], c_rows)
+    c_rows[me] = c_send[me]
+
+    def column(row):
+        return jnp.sum(jnp.where(eye, row[:, :rows], 0.0), axis=1, keepdims=True)
+
     loads[decay_i].wait()
     loads[beta_i].wait()
     decay_pre = dot_t(normed, w_decay[...])
@@ -185,19 +191,15 @@
         kq[:, heads + h, :] = q_unit
 
     def one_row(b, _):
-        columns = kq[b].T
+        pair = kq[b].astype(BF)
         for h in range(heads):
-            block = state[b, h]
-            recall[h, pl.ds(b, 1), :] = jnp.sum(columns[:, h : h + 1] * block, axis=0, keepdims=True)
-            recall[heads + h, pl.ds(b, 1), :] = jnp.sum(
-                columns[:, heads + h : heads + h + 1] * block, axis=0, keepdims=True
-            )
+            both = dot(pair, state[b, h].astype(BF))
+            recall[h, pl.ds(b, 1), :] = both[h : h + 1]
+            recall[heads + h, pl.ds(b, 1), :] = both[heads + h : heads + h + 1]
         return 0
 
-    lax.fori_loop(0, rows, one_row, 0)
+    lax.fori_loop(0, rows, one_row, 0, unroll=4)
     v_rows = summed(2)
-    wait_c = exchange(ep_copy, 4, ep_peers, me, lambda p: c_send.at[p], c_recv)
-    c_recv[me] = c_send[me]
     for h in range(heads):
         q_unit, k_unit = units[h]
         decay, beta = decays[h], betas[h]
@@ -205,9 +207,8 @@
         read = decay * recall[heads + h] + jnp.sum(q_unit * k_unit, axis=-1, keepdims=True) * corr
         read = read * lax.rsqrt(jnp.mean(read * read, axis=-1, keepdims=True) + EPS) * head_gain[...]
         head_out[:, h * 128 : (h + 1) * 128] = read.astype(BF)
-        key_out[:, h, :] = k_unit
-        corr_out[:, h, :] = corr
-        decay_out[:, h, :] = jnp.broadcast_to(decay, (rows, 128))
+        corr_ref[h] = corr
+        decay_ref[h] = jnp.broadcast_to(decay, (rows, 128))
 
     loads[o_i].wait()
     ho = head_out[...]
@@ -216,14 +217,29 @@
     wait_a = exchange(tp_copy, 0, tp_peers, my, lambda p: a_send.at[p], a_recv)
     a_recv[my] = a_send[my]
     own = pl.ds(pl.multiple_of(my * chunk, 128), chunk)
+
+    def update_row(b, _):
+        columns = kq[b].T
+        for h in range(heads):
+            corr = corr_ref[h, pl.ds(b, 1), :]
+            decay = decay_ref[h, pl.ds(b, 1), :]
+            state[b, h] = decay * state[b, h] + columns[:, h : h + 1] * corr
+        return 0
+
+    lax.fori_loop(0, rows, update_row, 0, unroll=2)
     middle = tokens[:, own].astype(F32)
     wait_a()
     for p in range(n_tp):
         middle = middle + a_recv[p].astype(F32)
+    x_all[me] = (middle * ffn_gain[:, own]).astype(BF)
+    for p in ep_peers:
+        ep_copy(5, x_all.at[me], x_all.at[me], p, me).start()
     middle_ref[...] = middle
     s_recv[my] = jnp.broadcast_to(jnp.sum(middle * middle, axis=-1, keepdims=True), (rows, 128))
     wait_s = exchange(tp_copy, 1, tp_peers, my, lambda p: s_recv.at[my], s_recv)
     wait_c()
+    for p in range(n_ep):
+        c_recv[p] = jnp.broadcast_to(column(c_rows[p, :1, :]), (rows, 128))
     tri = (
         lax.broadcasted_iota(jnp.int32, (group_tokens, group_tokens), 0)
         >= lax.broadcasted_iota(jnp.int32, (group_tokens, group_tokens), 1)
@@ -239,10 +255,14 @@
     total = s_recv[0]
     for p in range(1, n_tp):
         total = total + s_recv[p]
-    scale = lax.rsqrt(total[:, :1] / width + EPS)
-    x_all[me] = (middle * scale * ffn_gain[:, own]).astype(BF)
-    for p in ep_peers:
-        ep_copy(5, x_all.at[me], x_all.at[me], p, me).start()
+    scale = lax.rsqrt(total / width + EPS)
+    diagonal = lax.broadcasted_iota(jnp.int32, (rows, 128), 0) == lax.broadcasted_iota(
+        jnp.int32, (rows, 128), 1
+    )
+    scale_rows[me] = jnp.broadcast_to(
+        jnp.sum(jnp.where(diagonal, scale, 0.0), axis=0, keepdims=True), (8, 128)
+    )
+    wait_scale = exchange(ep_copy, 7, ep_peers, me, lambda p: scale_rows.at[me], scale_rows)
     wait_g = []
     for offset in range(groups):
         g = lax.rem(my_group - offset + groups, groups)
@@ -274,13 +294,28 @@
 
     for wait in wait_g:
         wait()
+    wait_scale()
+    for p in range(n_ep):
+        scale_ref[p] = jnp.broadcast_to(column(scale_rows[p, :1, :]), (rows, 128))
+    slot_scale = jnp.concatenate(
+        [
+            lax.dot_general(
+                place_ref[g].astype(F32),
+                scale_ref[g * members : (g + 1) * members].reshape(group_tokens, 128),
+                (((0,), (0,)), ((), ())), precision=lax.Precision.HIGHEST,
+                preferred_element_type=F32,
+            )
+            for g in range(groups)
+        ],
+        axis=0,
+    )[:, :1]
     gate = jnp.zeros((slots, w_eg.shape[2]), F32)
     up = jnp.zeros((slots, w_eg.shape[2]), F32)
     for c in range(n_tp):
         routed = g_all[c].astype(F32).reshape(slots, chunk).astype(BF)
         gate = gate + dot(routed, w_eg[0, c * chunk : (c + 1) * chunk, :])
         up = up + dot(routed, w_eu[0, c * chunk : (c + 1) * chunk, :])
-    expert_hidden = (silu(gate) * up).astype(BF)
+    expert_hidden = (silu(gate * slot_scale) * (up * slot_scale)).astype(BF)
     for c in range(n_tp):
         part = dot(expert_hidden, w_ed[0, :, c * chunk : (c + 1) * chunk])
         e_send[c] = part.reshape(groups, group_slots, chunk).astype(BF)
@@ -300,6 +335,8 @@
     pre = d_recv[0].astype(F32)
     for p in range(1, n_tp):
         pre = pre + d_recv[p].astype(F32)
+    per_part = part_rows // rows
+    pre = pre * scale_ref[pl.ds(my * per_part, per_part)].reshape(part_rows, 128)[:, :1]
     h_all[my] = (silu(pre[:, :hidden]) * pre[:, hidden:]).astype(BF)
     wait_h = exchange(tp_copy, 3, tp_peers, my, lambda p: h_all.at[my], h_all)
     for offset in returns[1:]:
@@ -364,16 +401,17 @@
     dims = (n_ep, n_tp, rows, width, heads, members, cap, len(small) + len(weights), len(weights))
     vmem = pl.BlockSpec(memory_space=pltpu.VMEM)
     kq_rows = -(-2 * heads // 8) * 8
-    scratch = [pltpu.VMEM(w.shape, w.dtype) for w in weights]
+    scratch = [pltpu.VMEM(w.shape, w.dtype) for w in weights[1:]]
     scratch += [
         pltpu.VMEM(shape, dtype)
         for shape, dtype in (
             ((n_ep, rows, depth), BF), ((n_ep, rows, depth), BF),
             ((3, n_ep, rows, local), BF), ((3, n_ep, rows, local), BF),
-            ((n_ep, rows, 128), F32), ((n_ep, rows, 128), F32),
-            ((rows, kq_rows, 128), F32), ((2 * heads, rows, 128), F32), ((rows, local), BF),
+            ((n_ep, 8, 128), F32), ((n_ep, 8, 128), F32), ((n_ep, rows, 128), F32),
+            ((rows, kq_rows, 128), F32), ((2 * heads, rows, 128), F32),
+            ((heads, rows, 128), F32), ((heads, rows, 128), F32), ((rows, local), BF),
             ((n_tp, rows, chunk), BF), ((n_tp, rows, chunk), BF), ((n_tp, rows, 128), F32),
-            ((rows, chunk), F32), ((n_ep, rows, chunk), BF), ((n_tp, groups, group_slots, chunk), BF),
+            ((n_ep, 8, 128), F32), ((n_ep, rows, 128), F32), ((rows, chunk), F32), ((n_ep, rows, chunk), BF), ((n_tp, groups, group_slots, chunk), BF),
             ((n_tp, batch // n_tp, 2 * hidden), BF), ((n_tp, batch // n_tp, 2 * hidden), BF),
             ((n_tp, batch // n_tp, hidden), BF),
             ((n_tp, groups, group_slots, chunk), BF), ((n_tp, groups, group_slots, chunk), BF),
@@ -383,21 +421,21 @@
     ]
     scratch += [
         pltpu.SemaphoreType.DMA((len(weights),)),
-        pltpu.SemaphoreType.DMA((7, n_ep)), pltpu.SemaphoreType.DMA((7, n_ep)),
+        pltpu.SemaphoreType.DMA((8, n_ep)), pltpu.SemaphoreType.DMA((8, n_ep)),
         pltpu.SemaphoreType.DMA((4 + 2 * groups, n_tp)), pltpu.SemaphoreType.DMA((4 + 2 * groups, n_tp)),
     ]
-    per_head = jax.ShapeDtypeStruct((rows, heads, 128), F32)
-    mixed_out, key, corr, decay = pl.pallas_call(
+    mixed_out, new_state = pl.pallas_call(
         functools.partial(kernel, dims),
-        out_shape=(jax.ShapeDtypeStruct((rows, chunk), BF), per_head, per_head, per_head),
+        out_shape=(
+            jax.ShapeDtypeStruct((rows, chunk), BF), pltpu.VMEM(delta_state.shape, F32),
+        ),
         in_specs=[vmem] * len(small) + [pl.BlockSpec(memory_space=pl.ANY)] * len(weights),
-        out_specs=(vmem,) * 4,
+        out_specs=(vmem, vmem),
         scratch_shapes=scratch,
         compiler_params=pltpu.CompilerParams(
-            collective_id=0, has_side_effects=True, vmem_limit_bytes=62 * 1024 * 1024
+            collective_id=0, has_side_effects=True, vmem_limit_bytes=44 * 1024 * 1024
         ),
     )(*small, *weights)
-    new_state = decay[:, :, None, :] * delta_state + key[..., :, None] * corr[..., None, :]
     return mixed_out, new_state
 
 

time: 87.2 us -> 85.3 us (0.978)
  local copies, waits for them, and re-layouts: 0.62 us -> 15.8 us
  Pallas kernels: 78.3 us -> 68.3 us
  other arithmetic: 7.37 us -> 0 us
    unnamed x3 -> x32, local copies, waits for them, and re-layouts: 0.62 us -> 15.8 us
    pallas_call x1, Pallas kernels: 78.3 us -> 68.3 us  [per_device(): pl.pallas_call(functools.partial(kernel, dims), out_shape=(jax.ShapeDtype...]
    add x1 -> x0, other arithmetic: 7.37 us -> none  [per_device(): decay[:, :, None, :] * delta_state + key[..., :, None] * corr[..., None, :]]
where the time goes in v1:
time: 85.3 us; the launch traced here: 84.8 us
  Pallas kernels  68.3 us (80%)
  local copies, waits for them, and re-layouts  15.8 us (19%)
    pallas_call x1, Pallas kernels, per_device(): pl.pallas_call(functools.partial(kernel, dims), out_shape=(jax.ShapeDtype...  68.3 us
    unnamed x32, local copies, waits for them, and re-layouts  15.8 us

profile of v1, /device:TPU:0, one launch (start us, length us, event | category | flops | bytes accessed | tf_op | source)
XLA Modules:
  0.0 84.8 jit_solution(11240902514628261601)
XLA Ops:
  0.6 0.0 copy-start
  0.6 1.2 %copy-done = bf16[1024,512]{1,0:T(8,128)(2,1)S(1)} copy-done((bf16[1024,512]{1,0:T(8,128)(2,1)S(1)}, bf16[1024,512]{1,0:T(8,128)(2,1)}, u32[]{:S(2)}) %copy-start) | copy-done | bytes 1048600
  1.9 0.0 copy-start.1
  1.9 1.0 %copy-done.1 = bf16[512,512]{1,0:T(8,128)(2,1)S(1)} copy-done((bf16[512,512]{1,0:T(8,128)(2,1)S(1)}, bf16[512,512]{1,0:T(8,128)(2,1)}, u32[]{:S(2)}) %copy-start.1) | copy-done | bytes 524312
  2.9 0.0 copy-start.2
  2.9 1.0 %copy-done.2 = bf16[512,512]{1,0:T(8,128)(2,1)S(1)} copy-done((bf16[512,512]{1,0:T(8,128)(2,1)S(1)}, bf16[512,512]{1,0:T(8,128)(2,1)}, u32[]{:S(2)}) %copy-start.2) | copy-done | bytes 524312
  3.9 0.0 copy-start.3
  4.0 1.0 %copy-done.3 = bf16[512,512]{1,0:T(8,128)(2,1)S(1)} copy-done((bf16[512,512]{1,0:T(8,128)(2,1)S(1)}, bf16[512,512]{1,0:T(8,128)(2,1)}, u32[]{:S(2)}) %copy-start.3) | copy-done | bytes 524312
  5.0 0.0 copy-start.4
  5.0 0.9 %copy-done.4 = bf16[24,4096]{1,0:T(8,128)(2,1)S(1)} copy-done((bf16[24,4096]{1,0:T(8,128)(2,1)S(1)}, bf16[24,4096]{1,0:T(8,128)(2,1)}, u32[]{:S(2)}) %copy-start.4) | copy-done | bytes 196632
  5.9 0.0 copy-start.5
  5.9 0.9 %copy-done.5 = bf16[4096,16]{0,1:T(8,128)(2,1)S(1)} copy-done((bf16[4096,16]{0,1:T(8,128)(2,1)S(1)}, bf16[4096,16]{0,1:T(8,128)(2,1)}, u32[]{:S(2)}) %copy-start.5) | copy-done | bytes 131096
  6.8 0.9 %copy-done.6 = bf16[4096,16]{0,1:T(8,128)(2,1)S(1)} copy-done((bf16[4096,16]{0,1:T(8,128)(2,1)S(1)}, bf16[4096,16]{0,1:T(8,128)(2,1)}, u32[]{:S(2)}) %copy-start.6) | copy-done | bytes 131096
  7.7 0.0 copy-start.7
  7.7 0.7 copy-done.7
  8.4 0.0 copy-start.8
  8.4 0.7 copy-done.8
  9.2 0.0 copy-start.9
  9.2 0.7 copy-done.9
  9.9 0.0 copy-start.10
  9.9 0.7 copy-done.10
  10.5 0.0 copy-start.11
  10.5 0.7 copy-done.11
  11.2 0.0 copy-start.12
  11.2 0.7 copy-done.12
  11.9 0.0 copy-start.13
  11.9 0.7 copy-done.13
  12.5 0.0 copy-start.14
  12.5 0.7 copy-done.14
  13.2 68.3 %shard_map.221 = (bf16[24,1024]{1,0:T(8,128)(2,1)S(1)}, f32[24,4,128,128]{3,2,1,0:T(8,128)S(1)}) custom-call(bf16[24,4096]{1,0:T(8,128)(2,1)S(1)} %copy-done.4, f32[1,4096]{1,0:T(1,128)S(1)} %bitcast.12, f32[1,4]{1,0:T(1,128)S(1)} %bitcast.17, f32[1,128]{1,0:T(1,128)S(1)} %bitcast.18, f32[1,4096]{1,0:T(1,128)S(1)} %bitcast.13, s32[2,24]{1,0:T(2,128)S(1)} %bitcast.15, ...), custom_call_target="tpu_custom_call" | custom-call | tf_op jit(solution)/shard_map/pallas_call | solution.py:427
  81.4 2.7 %copy.26 = f32[24,4,128,128]{3,2,1,0:T(8,128)} copy(f32[24,4,128,128]{3,2,1,0:T(8,128)S(1)} %get-tuple-element.3) | data formatting | bytes 12582912
  84.2 0.6 copy.27
  (1 shorter events, 0.0 us)
Async XLA Ops:
  0.6 1.2 %copy-start = (bf16[1024,512]{1,0:T(8,128)(2,1)S(1)}, bf16[1024,512]{1,0:T(8,128)(2,1)}, u32[]{:S(2)}) copy-start(bf16[1024,512]{1,0:T(8,128)(2,1)} %refs_16_.1) | copy-start | bytes 3145732
  1.9 1.0 %copy-start.1 = (bf16[512,512]{1,0:T(8,128)(2,1)S(1)}, bf16[512,512]{1,0:T(8,128)(2,1)}, u32[]{:S(2)}) copy-start(bf16[512,512]{1,0:T(8,128)(2,1)} %refs_12_.1) | copy-start | bytes 1572868
  2.9 1.0 %copy-start.2 = (bf16[512,512]{1,0:T(8,128)(2,1)S(1)}, bf16[512,512]{1,0:T(8,128)(2,1)}, u32[]{:S(2)}) copy-start(bf16[512,512]{1,0:T(8,128)(2,1)} %refs_13_.1) | copy-start | bytes 1572868
  3.9 1.0 %copy-start.3 = (bf16[512,512]{1,0:T(8,128)(2,1)S(1)}, bf16[512,512]{1,0:T(8,128)(2,1)}, u32[]{:S(2)}) copy-start(bf16[512,512]{1,0:T(8,128)(2,1)} %refs_14_.1) | copy-start | bytes 1572868
  5.0 0.9 %copy-start.4 = (bf16[24,4096]{1,0:T(8,128)(2,1)S(1)}, bf16[24,4096]{1,0:T(8,128)(2,1)}, u32[]{:S(2)}) copy-start(bf16[24,4096]{1,0:T(8,128)(2,1)} %refs_0_.1) | copy-start | bytes 589828
  5.9 0.9 %copy-start.5 = (bf16[4096,16]{0,1:T(8,128)(2,1)S(1)}, bf16[4096,16]{0,1:T(8,128)(2,1)}, u32[]{:S(2)}) copy-start(bf16[4096,16]{0,1:T(8,128)(2,1)} %param.28) | copy-start | bytes 393220
  6.8 0.9 %copy-start.6 = (bf16[4096,16]{0,1:T(8,128)(2,1)S(1)}, bf16[4096,16]{0,1:T(8,128)(2,1)}, u32[]{:S(2)}) copy-start(bf16[4096,16]{0,1:T(8,128)(2,1)} %param.29) | copy-start | bytes 393220
  7.7 0.7 copy-start.7
  8.4 0.7 copy-start.8
  9.2 0.7 copy-start.9
  9.9 0.7 copy-start.10
  10.5 0.7 copy-start.11
  11.2 0.7 copy-start.12
  11.9 0.7 copy-start.13
  12.5 0.7 copy-start.14

commit v2 on v1

--- a/solution.py
+++ b/solution.py
@@ -26,31 +26,18 @@
     return values / (1.0 + jnp.exp(-values))
 
 
-class BlockOf:
-    def __init__(self, ref, block):
-        self.ref, self.block = ref, block
-
-    @property
-    def at(self):
-        return self
-
-    def __getitem__(self, index):
-        return self.ref.at[index, self.block]
-
-
 def kernel(dims, *refs):
-    n_ep, n_tp, rows, width, heads, members, cap, n_in, n_weights = dims
-    inputs, refs = refs[:n_in], refs[n_in:]
-    (tokens, attn_gain, decay_rate, head_gain, ffn_gain, ids, group_prob, logit, mix) = inputs[:9]
-    hbm = inputs[9:]
+    n_ep, n_tp, rows, width, heads, members, cap, n_in = dims
+    hbm, refs = refs[:n_in], refs[n_in:]
     out, state = refs[:2]
-    held = (state,) + refs[2 : 1 + n_weights]
-    refs = refs[1 + n_weights :]
-    state, w_decay, w_beta, w_q, w_k, w_v, w_o, w_dg, w_du, w_eg, w_eu, w_ed, w_dd = held
+    held = refs[2 : 11] + (state,) + refs[11 : 1 + n_in]
+    refs = refs[1 + n_in :]
+    (tokens, attn_gain, decay_rate, head_gain, ffn_gain, ids, group_prob, logit, mix) = held[:9]
+    state, w_decay, w_beta, w_q, w_k, w_v, w_o, w_dg, w_du, w_eg, w_eu, w_ed, w_dd = held[9:]
     (
         n_send, n_recv, q_send, q_recv, c_send, c_rows, c_recv, kq, recall, corr_ref, decay_ref,
-        head_out, a_send, a_recv, s_recv, scale_rows, scale_ref, middle_ref, x_all, g_all, d_send, d_recv, h_all,
-        e_send, e_recv, f_send, f_recv, place_ref, dense_ref, load_sem, ep_send, ep_recv, tp_send, tp_recv,
+        head_out, a_send, a_recv, s_recv, scale_rows, scale_ref, middle_ref, x_all, g_all,
+        d_half, d_send, d_near, d_far, h_all, e_part, e_near, e_send, e_recv, f_send, f_recv, place_ref, dense_ref, load_sem, ep_send, ep_recv, tp_send, tp_recv,
     ) = refs
     me = lax.axis_index("ep")
     my = lax.axis_index("tp")
@@ -74,11 +61,13 @@
         pltpu.make_async_copy(src, dst, load_sem.at[i])
         for i, (src, dst) in enumerate(zip(hbm, held))
     ]
-    state_i, decay_i, beta_i, q_i, k_i, v_i, o_i, dg_i, du_i, eg_i, eu_i, ed_i, dd_i = range(13)
+    state_i, decay_i, beta_i, q_i, k_i, v_i, o_i, dg_i, du_i, eg_i, eu_i, ed_i, dd_i = range(9, 22)
     order = (decay_i, beta_i, q_i, k_i, v_i, state_i, o_i, dg_i, du_i, eg_i, eu_i, ed_i, dd_i)
 
     ep_peers = [p for offset in range(groups) for p in members_of(offset)]
     tp_peers = [lax.rem(my + d, n_tp) for d in range(1, n_tp)]
+    for i in range(9):
+        loads[i].start()
     barrier = pltpu.get_barrier_semaphore()
     for p in ep_peers:
         pl.semaphore_signal(barrier, inc=1, device_id=(p, my), device_id_type=MESH)
@@ -113,6 +102,8 @@
 
         return arrived
 
+    for i in range(9):
+        loads[i].wait()
     x = tokens[...].astype(F32)
     mean_sq = jnp.mean(x * x, axis=-1, keepdims=True)
     normed = (x * lax.rsqrt(mean_sq + EPS) * attn_gain[...]).astype(BF)
@@ -263,9 +254,44 @@
         jnp.sum(jnp.where(diagonal, scale, 0.0), axis=0, keepdims=True), (8, 128)
     )
     wait_scale = exchange(ep_copy, 7, ep_peers, me, lambda p: scale_rows.at[me], scale_rows)
-    wait_g = []
+    core = lax.rem(my, 2)
+    line = lax.div(my, 2)
+    lines = n_tp // 2
+    sibling = my + 1 - 2 * core
+    far_lines = [lax.rem(line + d, lines) for d in range(1, lines)]
+
+    def same_core(y):
+        return 2 * y + core
+
+    def other_core(y):
+        return 2 * y + 1 - core
+
+    def send_g(phase, g):
+        block = g_all.at[my, g]
+        tp_copy(phase, block, block, sibling, my).start()
+        for y in far_lines:
+            tp_copy(phase, block, block, same_core(y), my).start()
+
+    def pass_on(phase, g):
+        for y in far_lines:
+            block = g_all.at[same_core(y), g]
+            tp_copy(phase, block, block, same_core(y), same_core(y)).wait_recv()
+            pltpu.make_async_remote_copy(
+                src_ref=block, dst_ref=block,
+                send_sem=tp_send.at[phase, other_core(y)], recv_sem=tp_recv.at[phase, same_core(y)],
+                device_id=(me, sibling), device_id_type=MESH,
+            ).start()
+
+    def arrived_g(phase, g):
+        block = g_all.at[my, g]
+        for p in [sibling] + [other_core(y) for y in far_lines]:
+            tp_copy(phase, block, g_all.at[p, g], p, p).wait_recv()
+        for p in tp_peers:
+            tp_copy(phase, block, block, p, my).wait_send()
+
+    group_from = [lax.rem(my_group - offset + groups, groups) for offset in range(groups)]
     for offset in range(groups):
-        g = lax.rem(my_group - offset + groups, groups)
+        g = group_from[offset]
         for p in members_of(-offset):
             ep_copy(5, x_all.at[me], x_all.at[p], p, p).wait_recv()
         block = x_all[pl.ds(g * members, members)].astype(F32)
@@ -273,27 +299,29 @@
             place_ref[g], block.reshape(group_tokens, chunk).astype(BF),
             (((0,), (0,)), ((), ())), preferred_element_type=F32,
         ).astype(BF)
-        wait_g.append(
-            exchange(
-                tp_copy, 4 + offset, tp_peers, my, lambda p, g=g: g_all.at[my, g],
-                BlockOf(g_all, g),
-            )
-        )
-    for p in ep_peers:
-        ep_copy(5, x_all.at[me], x_all.at[me], p, me).wait_send()
+        send_g(4 + offset, g)
+        if offset > 1:
+            pass_on(2 + offset, group_from[offset - 2])
     for i in (dg_i, du_i, eg_i, eu_i, ed_i, dd_i):
         loads[i].wait()
     xs = x_all[...].astype(F32).reshape(batch, chunk).astype(BF)
     hidden = w_dg.shape[1]
-    part_rows = batch // n_tp
+    half_rows = batch // 2
     for j, w in enumerate((w_dg, w_du)):
-        part = dot(xs, w[...]).reshape(n_tp, part_rows, hidden)
-        d_send[:, :, j * hidden : (j + 1) * hidden] = part.astype(BF)
-    wait_d = exchange(tp_copy, 2, tp_peers, my, lambda p: d_send.at[p], d_recv)
-    d_recv[my] = d_send[my]
-
-    for wait in wait_g:
-        wait()
+        d_half[:, :, j * hidden : (j + 1) * hidden] = dot(xs, w[...]).reshape(2, half_rows, hidden)
+    d_send[1] = d_half[1 - core].astype(BF)
+    near_d = tp_copy(2, d_send.at[1], d_near, sibling, sibling)
+    tp_copy(2, d_send.at[1], d_near, sibling, my).start()
+    if groups > 1:
+        pass_on(2 + groups, group_from[groups - 2])
+    near_d.wait_recv()
+    pre = d_half[core] + d_near[...].astype(F32)
+    d_half[0] = pre
+    d_send[0] = pre.astype(BF)
+    for y in far_lines:
+        tp_copy(3, d_send.at[0], d_far.at[line], same_core(y), my).start()
+    for p in ep_peers:
+        ep_copy(5, x_all.at[me], x_all.at[me], p, me).wait_send()
     wait_scale()
     for p in range(n_ep):
         scale_ref[p] = jnp.broadcast_to(column(scale_rows[p, :1, :]), (rows, 128))
@@ -309,6 +337,9 @@
         ],
         axis=0,
     )[:, :1]
+    pass_on(3 + groups, group_from[groups - 1])
+    for offset in range(groups):
+        arrived_g(4 + offset, group_from[offset])
     gate = jnp.zeros((slots, w_eg.shape[2]), F32)
     up = jnp.zeros((slots, w_eg.shape[2]), F32)
     for c in range(n_tp):
@@ -316,48 +347,69 @@
         gate = gate + dot(routed, w_eg[0, c * chunk : (c + 1) * chunk, :])
         up = up + dot(routed, w_eu[0, c * chunk : (c + 1) * chunk, :])
     expert_hidden = (silu(gate * slot_scale) * (up * slot_scale)).astype(BF)
-    for c in range(n_tp):
-        part = dot(expert_hidden, w_ed[0, :, c * chunk : (c + 1) * chunk])
-        e_send[c] = part.reshape(groups, group_slots, chunk).astype(BF)
-    e_recv[my] = e_send[my]
+    for y in range(lines):
+        for c in range(2):
+            at = (2 * y + c) * chunk
+            part = dot(expert_hidden, w_ed[0, :, at : at + chunk])
+            e_part[c, :, y] = part.reshape(groups, group_slots, chunk).astype(BF)
     returns = list(range(1, groups)) + [0]
     group_at = [lax.rem(my_group + offset, groups) for offset in range(groups)]
 
-    def send_e(offset):
+    def near_e(offset, source):
         g = group_at[offset]
-        return exchange(
-            tp_copy, 4 + groups + offset, tp_peers, my, lambda p: e_send.at[p, g],
-            BlockOf(e_recv, g),
+        return tp_copy(
+            4 + groups + offset, e_part.at[1 - core, g], e_near.at[g], sibling, source
         )
 
-    wait_e = {returns[0]: send_e(returns[0])}
-    wait_d()
-    pre = d_recv[0].astype(F32)
-    for p in range(1, n_tp):
-        pre = pre + d_recv[p].astype(F32)
-    per_part = part_rows // rows
-    pre = pre * scale_ref[pl.ds(my * per_part, per_part)].reshape(part_rows, 128)[:, :1]
-    h_all[my] = (silu(pre[:, :hidden]) * pre[:, hidden:]).astype(BF)
-    wait_h = exchange(tp_copy, 3, tp_peers, my, lambda p: h_all.at[my], h_all)
-    for offset in returns[1:]:
-        wait_e[offset] = send_e(offset)
-    wait_h()
+    def far_e(offset, y, source):
+        g = group_at[offset]
+        return tp_copy(
+            4 + 2 * groups + offset, e_send.at[g, y], e_recv.at[g, lax.div(source, 2)], same_core(y), source
+        )
+
+    for offset in returns:
+        near_e(offset, my).start()
+
+    for y in far_lines:
+        tp_copy(3, d_send.at[0], d_far.at[y], same_core(y), same_core(y)).wait_recv()
+    pre = d_half[0]
+    for y in far_lines:
+        pre = pre + d_far[y].astype(F32)
+    half_blocks = n_ep // 2
+    pre = pre * scale_ref[pl.ds(core * half_blocks, half_blocks)].reshape(half_rows, 128)[:, :1]
+    h_all[core] = (silu(pre[:, :hidden]) * pre[:, hidden:]).astype(BF)
+    tp_copy(4 + 3 * groups, h_all.at[core], h_all.at[core], sibling, my).start()
+    for offset in returns:
+        g = group_at[offset]
+        near_e(offset, sibling).wait_recv()
+        for y in far_lines:
+            e_send[g, y] = (e_part[core, g, y].astype(F32) + e_near[g, y].astype(F32)).astype(BF)
+            far_e(offset, y, my).start()
+    tp_copy(4 + 3 * groups, h_all.at[core], h_all.at[1 - core], sibling, sibling).wait_recv()
     dense_hidden = h_all[...].astype(F32).reshape(batch, hidden).astype(BF)
     dense = dot(dense_hidden, w_dd[...]) * (1.0 / (1.0 + jnp.exp(-mix[...])))
     dense_ref[...] = dense.reshape(n_ep, rows, chunk)
     for offset in returns:
         g = group_at[offset]
         here = pl.ds(g * members, members)
-        wait_e[offset]()
-        result = e_recv[0, g].astype(F32)
-        for p in range(1, n_tp):
-            result = result + e_recv[p, g].astype(F32)
+        result = e_part[core, g, line].astype(F32) + e_near[g, line].astype(F32)
+        for y in far_lines:
+            far_e(offset, y, same_core(y)).wait_recv()
+            result = result + e_recv[g, y].astype(F32)
         coef = c_recv[here].reshape(group_tokens, 128)[:, :1]
         mixed = coef * dot(place_ref[g], result.astype(BF))
         combined = dense_ref[here] + mixed.reshape(members, rows, chunk)
         f_send[here] = combined.astype(BF)
         for p in members_of(offset):
             ep_copy(6, f_send.at[p], f_recv.at[me], p, me).start()
+    tp_copy(2, d_send.at[1], d_near, sibling, my).wait_send()
+    tp_copy(4 + 3 * groups, h_all.at[core], h_all.at[core], sibling, sibling).wait_send()
+    for y in far_lines:
+        tp_copy(3, d_send.at[0], d_far.at[line], same_core(y), my).wait_send()
+    for offset in range(groups):
+        near_e(offset, my).wait_send()
+        for y in far_lines:
+            far_e(offset, y, my).wait_send()
     final = middle_ref[...] + f_send[me].astype(F32)
     f_recv[me] = jnp.zeros((rows, chunk), BF)
     for p in ep_peers:
@@ -398,10 +450,11 @@
         delta_state, decay_weight.T, beta_weight.T, query_weight, key_weight, value_weight,
         output_weight, dense_gate, dense_up, expert_gate, expert_up, expert_down, dense_down,
     )
-    dims = (n_ep, n_tp, rows, width, heads, members, cap, len(small) + len(weights), len(weights))
+    arrays = tuple(pltpu.with_memory_space_constraint(a, pltpu.HBM) for a in small + weights)
+    dims = (n_ep, n_tp, rows, width, heads, members, cap, len(arrays))
     vmem = pl.BlockSpec(memory_space=pltpu.VMEM)
     kq_rows = -(-2 * heads // 8) * 8
-    scratch = [pltpu.VMEM(w.shape, w.dtype) for w in weights[1:]]
+    scratch = [pltpu.VMEM(a.shape, a.dtype) for a in small + weights[1:]]
     scratch += [
         pltpu.VMEM(shape, dtype)
         for shape, dtype in (
@@ -412,30 +465,34 @@
             ((heads, rows, 128), F32), ((heads, rows, 128), F32), ((rows, local), BF),
             ((n_tp, rows, chunk), BF), ((n_tp, rows, chunk), BF), ((n_tp, rows, 128), F32),
             ((n_ep, 8, 128), F32), ((n_ep, rows, 128), F32), ((rows, chunk), F32), ((n_ep, rows, chunk), BF), ((n_tp, groups, group_slots, chunk), BF),
-            ((n_tp, batch // n_tp, 2 * hidden), BF), ((n_tp, batch // n_tp, 2 * hidden), BF),
-            ((n_tp, batch // n_tp, hidden), BF),
-            ((n_tp, groups, group_slots, chunk), BF), ((n_tp, groups, group_slots, chunk), BF),
+            ((2, batch // 2, 2 * hidden), F32), ((2, batch // 2, 2 * hidden), BF),
+            ((batch // 2, 2 * hidden), BF), ((n_tp // 2, batch // 2, 2 * hidden), BF),
+            ((2, batch // 2, hidden), BF),
+            ((2, groups, n_tp // 2, group_slots, chunk), BF),
+            ((groups, n_tp // 2, group_slots, chunk), BF),
+            ((groups, n_tp // 2, group_slots, chunk), BF),
+            ((groups, n_tp // 2, group_slots, chunk), BF),
             ((n_ep, rows, chunk), BF), ((n_ep, rows, chunk), BF),
             ((groups, members * rows, group_slots), BF), ((n_ep, rows, chunk), F32),
         )
     ]
     scratch += [
-        pltpu.SemaphoreType.DMA((len(weights),)),
+        pltpu.SemaphoreType.DMA((len(arrays),)),
         pltpu.SemaphoreType.DMA((8, n_ep)), pltpu.SemaphoreType.DMA((8, n_ep)),
-        pltpu.SemaphoreType.DMA((4 + 2 * groups, n_tp)), pltpu.SemaphoreType.DMA((4 + 2 * groups, n_tp)),
+        pltpu.SemaphoreType.DMA((5 + 3 * groups, n_tp)), pltpu.SemaphoreType.DMA((5 + 3 * groups, n_tp)),
     ]
     mixed_out, new_state = pl.pallas_call(
         functools.partial(kernel, dims),
         out_shape=(
             jax.ShapeDtypeStruct((rows, chunk), BF), pltpu.VMEM(delta_state.shape, F32),
         ),
-        in_specs=[vmem] * len(small) + [pl.BlockSpec(memory_space=pl.ANY)] * len(weights),
+        in_specs=[pl.BlockSpec(memory_space=pltpu.HBM)] * len(arrays),
         out_specs=(vmem, vmem),
         scratch_shapes=scratch,
         compiler_params=pltpu.CompilerParams(
             collective_id=0, has_side_effects=True, vmem_limit_bytes=44 * 1024 * 1024
         ),
-    )(*small, *weights)
+    )(*arrays)
     return mixed_out, new_state
 
 

time: 85.3 us -> 69.7 us (0.82)
  local copies, waits for them, and re-layouts: 15.8 us -> 3.33 us
  Pallas kernels: 68.3 us -> 65.6 us
    unnamed x32 -> x2, local copies, waits for them, and re-layouts: 15.8 us -> 3.33 us
    pallas_call x1, Pallas kernels: 68.3 us -> 65.6 us  [per_device(): pl.pallas_call(functools.partial(kernel, dims), out_shape=(jax.ShapeDtype...]
where the time goes in v2:
time: 69.7 us; the launch traced here: 69.5 us
  Pallas kernels  65.6 us (94%)
  local copies, waits for them, and re-layouts  3.33 us (5%)
    pallas_call x1, Pallas kernels, per_device(): pl.pallas_call(functools.partial(kernel, dims), out_shape=(jax.ShapeDtype...  65.6 us
    unnamed x2, local copies, waits for them, and re-layouts  3.33 us

profile of v2, /device:TPU:0, one launch (start us, length us, event | category | flops | bytes accessed | tf_op | source)
XLA Modules:
  0.0 69.5 jit_solution(10771971651867702989)
XLA Ops:
  0.6 65.6 %shard_map.221 = (bf16[24,1024]{1,0:T(8,128)(2,1)S(1)}, f32[24,4,128,128]{3,2,1,0:T(8,128)S(1)}) custom-call(bf16[24,4096]{1,0:T(8,128)(2,1)} %refs_0_.1, f32[1,4096]{1,0:T(1,128)} %bitcast.12, f32[1,4]{1,0:T(1,128)} %bitcast.17, f32[1,128]{1,0:T(1,128)} %bitcast.18, f32[1,4096]{1,0:T(1,128)} %bitcast.13, s32[2,24]{1,0:T(2,128)} %bitcast.15, ...), custom_call_target="tpu_custom_call" | custom-call | tf_op jit(solution)/shard_map/pallas_call | solution.py:484
  66.2 2.7 %copy.26 = f32[24,4,128,128]{3,2,1,0:T(8,128)} copy(f32[24,4,128,128]{3,2,1,0:T(8,128)S(1)} %get-tuple-element.3) | data formatting | bytes 12582912
  68.9 0.6 copy.27

commit v3 on v2

v3 whole, which is shorter than its diff:
```python
import functools
import math

import jax
import jax.numpy as jnp
from jax import lax
from jax.experimental import pallas as pl
from jax.experimental.pallas import tpu as pltpu
from jax.sharding import PartitionSpec as P

EPS = 1e-06
BF = jnp.bfloat16
F32 = jnp.float32
MESH = pl.DeviceIdType.MESH


def dot(left, right):
    return jnp.dot(left, right, preferred_element_type=F32)


def dot_t(left, right):
    return lax.dot_general(left, right, (((1,), (1,)), ((), ())), preferred_element_type=F32)


def silu(values):
    return values / (1.0 + jnp.exp(-values))


def far_first(position, count):
    low = 1 - lax.div(2 * position, count)
    order = []
    for k in range(count - 1):
        down = count - 1 - k
        down = down - lax.div(position - down + count, count)
        up = k + lax.div(k - position + count, count)
        order.append(low * down + (1 - low) * up)
    return order


def store_kernel(state, mixed, state_out, mixed_out, sems):
    rows = state.shape[0]
    copies = [pltpu.make_async_copy(mixed, mixed_out, sems.at[rows])]
    copies += [
        pltpu.make_async_copy(state.at[r], state_out.at[r], sems.at[r]) for r in range(rows)
    ]
    for copy in copies:
        copy.start()
    for copy in copies:
        copy.wait()


def semaphores(n_ep, n_tp, groups, n_in):
    pairs, lines = n_ep // 2, n_tp // 2
    sizes = {
        "load": n_in, "ns": 1, "nr": 1, "cs": 1, "cr": 1, "zs": 1, "zr": 1,
        "q1s": 1, "q1r": 3, "q2s": 1, "q2r": 3, "xs": 1, "xr": n_ep,
        "f1s": 1, "f1r": groups, "f2s": 1, "f2r": pairs, "as": 1, "ar": 1, "ss": 1, "sr": 1,
        "d1s": 1, "d1r": 1, "d2s": 1, "d2r": lines, "hs": 1, "hr": 1,
        "gs": 1, "gr": groups * n_tp, "e1s": 1, "e1r": groups, "e2s": 1, "e2r": groups,
    }
    starts, total = {}, 0
    for name, size in sizes.items():
        starts[name] = total
        total += size
    return starts, total


def kernel(dims, *refs):
    n_ep, n_tp, rows, width, heads, members, cap, n_in, starts = dims
    hbm, refs = refs[:n_in], refs[n_in:]
    out, state = refs[:2]
    held = refs[2 : 11] + (state,) + refs[11 : 1 + n_in]
    refs = refs[1 + n_in :]
    (tokens, attn_gain, decay_rate, head_gain, ffn_gain, ids, group_prob, logit, mix) = held[:9]
    state, w_decay, w_beta, w_q, w_k, w_v, w_o, w_dg, w_du, w_eg, w_eu, w_ed, w_dd = held[9:]
    (
        n_send, n_recv, q_away, q_mate, q_own, q_send, q_recv, c_send, c_rows, c_recv, kq, recall,
        corr_ref, decay_ref, head_out, a_send, a_recv, s_recv, scale_rows, scale_ref, middle_ref,
        x_all, g_all, d_half, d_send, d_near, d_far, h_all, e_part, e_near, e_send, e_recv,
        comb, f_away, f_mate, f_send, f_recv, place_ref, dense_ref, sems,
    ) = refs
    me = lax.axis_index("ep")
    my = lax.axis_index("tp")
    chunk = width // n_tp
    depth = width // n_ep
    batch = n_ep * rows
    local = heads * 128
    groups = n_ep // members
    group_slots = members * cap
    group_tokens = members * rows
    slots = groups * group_slots
    pairs = n_ep // 2
    lines = n_tp // 2
    group_pairs = members // 2
    pair = lax.div(me, 2)
    par = lax.rem(me, 2)
    mate = me + 1 - 2 * par
    core = lax.rem(my, 2)
    line = lax.div(my, 2)
    sibling = my + 1 - 2 * core
    my_group = lax.div(pair, group_pairs)
    far_groups = far_first(my_group, groups)
    far_lines = [lax.rem(line + d, lines) for d in range(1, lines)]

    def same_core(y):
        return 2 * y + core

    def other_core(y):
        return 2 * y + 1 - core

    def twin(q):
        return 2 * q + par

    def cross(q):
        return 2 * q + 1 - par

    def pairs_in(g, own=False):
        mine = lax.rem(pair, group_pairs)
        return [
            g * group_pairs + lax.rem(mine + m, group_pairs)
            for m in range(1 if own else 0, group_pairs)
        ]

    others = [q for g in far_groups for q in pairs_in(g)] + pairs_in(my_group, True)
    ep_peers = [p for q in others for p in (cross(q), twin(q))] + [mate]
    far_tp = [p for y in far_lines for p in (same_core(y), other_core(y))]
    tp_peers = far_tp + [sibling]

    def sem(name, index=0):
        return sems.at[starts[name] + index]

    def ep_copy(src, dst, name, peer, index=0):
        return pltpu.make_async_remote_copy(
            src_ref=src, dst_ref=dst, send_sem=sem(name + "s"), recv_sem=sem(name + "r", index),
            device_id=(peer, my), device_id_type=MESH,
        )

    def tp_copy(src, dst, name, peer, index=0):
        return pltpu.make_async_remote_copy(
            src_ref=src, dst_ref=dst, send_sem=sem(name + "s"), recv_sem=sem(name + "r", index),
            device_id=(me, peer), device_id_type=MESH,
        )

    drains = []

    loads = [
        pltpu.make_async_copy(src, dst, sem("load", i))
        for i, (src, dst) in enumerate(zip(hbm, held))
    ]
    state_i, decay_i, beta_i, q_i, k_i, v_i, o_i, dg_i, du_i, eg_i, eu_i, ed_i, dd_i = range(9, 22)
    order = (decay_i, beta_i, k_i, q_i, v_i, state_i, o_i, dg_i, du_i, eg_i, eu_i, ed_i, dd_i)
    for i in range(9):
        loads[i].start()
    barrier = pltpu.get_barrier_semaphore()
    for p in ep_peers:
        pl.semaphore_signal(barrier, inc=1, device_id=(p, my), device_id_type=MESH)
    for p in tp_peers:
        pl.semaphore_signal(barrier, inc=1, device_id=(me, p), device_id_type=MESH)
    for i in order:
        loads[i].start()

    for i in range(9):
        loads[i].wait()
    x = tokens[...].astype(F32)
    mean_sq = jnp.mean(x * x, axis=-1, keepdims=True)
    normed = (x * lax.rsqrt(mean_sq + EPS) * attn_gain[...]).astype(BF)
    for p in range(n_ep):
        n_send[p] = normed[:, p * depth : (p + 1) * depth]
    pl.semaphore_wait(barrier, n_ep + n_tp - 2)
    here = par * pairs + pair
    for p in ep_peers:
        ep_copy(n_send.at[p], n_recv.at[here], "n", p).start()
    n_recv[here] = n_send[me]

    logit_exp = jnp.exp(logit[...])
    route = group_prob[...] * logit_exp / jnp.sum(logit_exp, axis=0, keepdims=True)
    names = ids[...]
    eye = lax.broadcasted_iota(jnp.int32, (rows, rows), 0) == lax.broadcasted_iota(
        jnp.int32, (rows, rows), 1
    )
    c_send[...] = jnp.zeros_like(c_send)
    for p in range(n_ep):
        flat = jnp.sum(jnp.where(names == p, route, 0.0), axis=0, keepdims=True)
        c_send[p, :, :rows] = jnp.broadcast_to(flat, (8, rows))
    for p in ep_peers:
        ep_copy(c_send.at[p], c_rows.at[me], "c", p).start()
    c_rows[me] = c_send[me]

    def column(row):
        return jnp.sum(jnp.where(eye, row[:, :rows], 0.0), axis=1, keepdims=True)

    loads[decay_i].wait()
    loads[beta_i].wait()
    decay_pre = dot_t(normed, w_decay[...])
    beta_pre = dot_t(normed, w_beta[...])
    lane = lax.broadcasted_iota(jnp.int32, decay_pre.shape, 1)
    decays, betas = [], []
    for h in range(heads):
        mine = lane == my * heads + h
        d = jnp.sum(jnp.where(mine, decay_pre, 0.0), axis=1, keepdims=True)
        b = jnp.sum(jnp.where(mine, beta_pre, 0.0), axis=1, keepdims=True)
        soft = jnp.maximum(d, 0.0) + jnp.log1p(jnp.exp(-jnp.abs(d)))
        decays.append(jnp.exp(-decay_rate[:, h : h + 1] * soft))
        betas.append(1.0 / (1.0 + jnp.exp(-b)))
    for i in (q_i, k_i, v_i):
        loads[i].wait()

    most = pl.ds(0, n_ep - 1)
    done_n = ep_copy(n_send.at[most], n_recv.at[most], "n", mate)
    done_n.wait_recv()
    drains.append(done_n)

    def rows_of(parity):
        held_rows = n_recv[pl.ds(parity * pairs, pairs)].astype(F32)
        return held_rows.reshape(pairs * rows, depth).astype(BF)

    away, near = rows_of(1 - par), rows_of(par)
    for j, w in enumerate((w_k, w_q, w_v)):
        q_away[j] = dot(away, w[...]).reshape(pairs, rows, local).astype(BF)
        ep_copy(q_away.at[j], q_mate.at[j], "q1", mate, j).start()
    for j, w in enumerate((w_k, w_q, w_v)):
        q_own[j] = dot(near, w[...]).reshape(pairs, rows, local)
    for j in range(3):
        ep_copy(q_away.at[j], q_mate.at[j], "q1", mate, j).wait_recv()
        both = q_own[j] + q_mate[j].astype(F32)
        q_own[j] = both
        q_send[j] = both.astype(BF)
        for q in others:
            ep_copy(q_send.at[j, q], q_recv.at[j, pair], "q2", twin(q), j).start()
    drains.append(ep_copy(q_away, q_mate, "q1", mate))
    far_blocks = pl.ds(0, pairs - 1)
    sent = q_send.at[pl.ds(0, 3), far_blocks]
    drains.append(ep_copy(sent, q_recv.at[pl.ds(0, 3), far_blocks], "q2", mate))

    def summed(j):
        ep_copy(
            q_send.at[j, far_blocks], q_recv.at[j, far_blocks], "q2", mate, j
        ).wait_recv()
        total = q_own[j, pair]
        for q in others:
            total = total + q_recv[j, q].astype(F32)
        return total.astype(BF).astype(F32)

    k_rows = summed(0)
    q_rows = summed(1)
    loads[state_i].wait()

    def head_of(values, h):
        return values[:, h * 128 : (h + 1) * 128]

    def unit(values):
        return values * lax.rsqrt(jnp.sum(values * values, axis=-1, keepdims=True) + EPS)

    units = []
    for h in range(heads):
        q_unit = unit(head_of(q_rows, h)) * 128 ** (-0.5)
        k_unit = unit(head_of(k_rows, h))
        units.append((q_unit, k_unit))
        kq[:, h, :] = k_unit
        kq[:, heads + h, :] = q_unit

    def one_row(b, _):
        both = kq[b].astype(BF)
        for h in range(heads):
            read = dot(both, state[b, h].astype(BF))
            recall[h, pl.ds(b, 1), :] = read[h : h + 1]
            recall[heads + h, pl.ds(b, 1), :] = read[heads + h : heads + h + 1]
        return 0

    lax.fori_loop(0, rows, one_row, 0, unroll=4)
    v_rows = summed(2)
    for h in range(heads):
        q_unit, k_unit = units[h]
        decay, beta = decays[h], betas[h]
        corr = beta * (head_of(v_rows, h) - decay * recall[h])
        read = decay * recall[heads + h] + jnp.sum(q_unit * k_unit, axis=-1, keepdims=True) * corr
        read = read * lax.rsqrt(jnp.mean(read * read, axis=-1, keepdims=True) + EPS) * head_gain[...]
        head_out[:, h * 128 : (h + 1) * 128] = read.astype(BF)
        corr_ref[h] = corr
        decay_ref[h] = jnp.broadcast_to(decay, (rows, 128))

    loads[o_i].wait()
    ho = head_out[...]

    def columns_of(p):
        return pl.ds(pl.multiple_of(p * chunk, 128), chunk)

    for p in far_tp + [sibling]:
        a_send[p] = dot(ho, w_o[:, columns_of(p)]).astype(BF)
        tp_copy(a_send.at[p], a_recv.at[my], "a", p).start()
    a_recv[my] = dot(ho, w_o[:, columns_of(my)]).astype(BF)
    own = columns_of(my)

    def update_row(b, _):
        columns = kq[b].T
        for h in range(heads):
            corr = corr_ref[h, pl.ds(b, 1), :]
            decay = decay_ref[h, pl.ds(b, 1), :]
            state[b, h] = decay * state[b, h] + columns[:, h : h + 1] * corr
        return 0

    lax.fori_loop(0, rows // 2, update_row, 0, unroll=4)
    middle = tokens[:, own].astype(F32)
    most_tp = pl.ds(0, n_tp - 1)
    done_a = tp_copy(a_send.at[most_tp], a_recv.at[most_tp], "a", sibling)
    done_a.wait_recv()
    drains.append(done_a)
    for p in range(n_tp):
        middle = middle + a_recv[p].astype(F32)
    x_all[me] = (middle * ffn_gain[:, own]).astype(BF)
    for p in [mate] + [twin(q) for q in others]:
        ep_copy(x_all.at[me], x_all.at[me], "x", p, me).start()
    middle_ref[...] = middle
    s_recv[my] = jnp.broadcast_to(jnp.sum(middle * middle, axis=-1, keepdims=True), (rows, 128))
    for p in tp_peers:
        tp_copy(s_recv.at[my], s_recv.at[my], "s", p).start()
    lax.fori_loop(rows // 2, rows, update_row, 0, unroll=4)
    done_c = ep_copy(c_send.at[most], c_rows.at[most], "c", mate)
    done_c.wait_recv()
    drains.append(done_c)
    for p in range(n_ep):
        c_recv[p] = jnp.broadcast_to(column(c_rows[p, :1, :]), (rows, 128))
    tri = (
        lax.broadcasted_iota(jnp.int32, (group_tokens, group_tokens), 0)
        >= lax.broadcasted_iota(jnp.int32, (group_tokens, group_tokens), 1)
    ).astype(F32).astype(BF)
    slot = lax.broadcasted_iota(jnp.int32, (group_tokens, group_slots), 1).astype(F32)
    for g in range(groups):
        coef = c_recv[g * members : (g + 1) * members].reshape(group_tokens, 128)[:, :1]
        named = coef > 0.0
        flags = jnp.broadcast_to(jnp.where(named, 1.0, 0.0), (group_tokens, 128)).astype(BF)
        rank = dot(tri, flags)[:, :1] - 1.0
        place_ref[g] = jnp.where((rank == slot) & named, 1.0, 0.0).astype(BF)
    done_s = tp_copy(s_recv.at[most_tp], s_recv.at[most_tp], "s", sibling)
    done_s.wait_recv()
    drains.append(done_s)
    total = s_recv[0]
    for p in range(1, n_tp):
        total = total + s_recv[p]
    scale = lax.rsqrt(total / width + EPS)
    diagonal = lax.broadcasted_iota(jnp.int32, (rows, 128), 0) == lax.broadcasted_iota(
        jnp.int32, (rows, 128), 1
    )
    scale_rows[me] = jnp.broadcast_to(
        jnp.sum(jnp.where(diagonal, scale, 0.0), axis=0, keepdims=True), (8, 128)
    )
    for p in ep_peers:
        ep_copy(scale_rows.at[me], scale_rows.at[me], "z", p).start()

    def send_g(k, g):
        block = g_all.at[my, g]
        for p in [same_core(y) for y in far_lines] + [sibling]:
            tp_copy(block, block, "g", p, k * n_tp + my).start()

    def pass_on(k, g):
        for y in far_lines:
            p = same_core(y)
            block = g_all.at[p, g]
            tp_copy(block, block, "g", p, k * n_tp + p).wait_recv()
            tp_copy(block, block, "g", sibling, k * n_tp + p).start()

    def arrived_g(k, g, p):
        block = g_all.at[p, g]
        tp_copy(block, block, "g", p, k * n_tp + p).wait_recv()

    def forward_x(g, own_group):
        for q in pairs_in(g, own_group):
            block = x_all.at[twin(q)]
            ep_copy(block, block, "x", twin(q), twin(q)).wait_recv()
            ep_copy(block, block, "x", mate, twin(q)).start()

    group_from = [my_group] + far_groups
    forward_x(my_group, True)
    for k in range(groups):
        g = group_from[k]
        if k + 1 < groups:
            forward_x(group_from[k + 1], False)
        for q in pairs_in(g, k == 0) + ([pair] if k == 0 else []):
            ep_copy(x_all.at[me], x_all.at[cross(q)], "x", mate, cross(q)).wait_recv()
        block = x_all[pl.ds(g * members, members)].astype(F32)
        g_all[my, g] = lax.dot_general(
            place_ref[g], block.reshape(group_tokens, chunk).astype(BF),
            (((0,), (0,)), ((), ())), preferred_element_type=F32,
        ).astype(BF)
        send_g(k, g)
        if k > 1:
            pass_on(k - 2, group_from[k - 2])
    drains.append(ep_copy(x_all.at[most], x_all.at[most], "x", mate))
    drains.append(tp_copy(g_all.at[most_tp], g_all.at[most_tp], "g", sibling))
    for i in (dg_i, du_i, eg_i, eu_i, ed_i, dd_i):
        loads[i].wait()
    xs = x_all[...].astype(F32).reshape(batch, chunk).astype(BF)
    hidden = w_dg.shape[1]
    half_rows = batch // 2
    for j, w in enumerate((w_dg, w_du)):
        d_half[:, :, j * hidden : (j + 1) * hidden] = dot(xs, w[...]).reshape(2, half_rows, hidden)
    d_send[1] = d_half[1 - core].astype(BF)
    near_d = tp_copy(d_send.at[1], d_near, "d1", sibling)
    near_d.start()
    drains.append(near_d)
    if groups > 1:
        pass_on(groups - 2, group_from[groups - 2])

    def expert_in(p, gate, up):
        routed = g_all[p].astype(F32).reshape(slots, chunk).astype(BF)
        return (
            gate + dot(routed, w_eg[0, columns_of(p), :]), up + dot(routed, w_eu[0, columns_of(p), :])
        )

    gate = jnp.zeros((slots, w_eg.shape[2]), F32)
    gate, up = expert_in(my, gate, gate)
    for k in range(groups):
        arrived_g(k, group_from[k], sibling)
    gate, up = expert_in(sibling, gate, up)
    near_d.wait_recv()
    pre = d_half[core] + d_near[...].astype(F32)
    d_half[0] = pre
    d_send[0] = pre.astype(BF)
    for y in far_lines:
        tp_copy(d_send.at[0], d_far.at[line], "d2", same_core(y), line).start()
    for y in far_lines:
        drains.append(tp_copy(d_send.at[0], d_far.at[line], "d2", same_core(y), line))
    pass_on(groups - 1, group_from[groups - 1])
    done_z = ep_copy(scale_rows.at[most], scale_rows.at[most], "z", mate)
    done_z.wait_recv()
    drains.append(done_z)
    for p in range(n_ep):
        scale_ref[p] = jnp.broadcast_to(column(scale_rows[p, :1, :]), (rows, 128))
    slot_scale = jnp.concatenate(
        [
            lax.dot_general(
                place_ref[g].astype(F32),
                scale_ref[g * members : (g + 1) * members].reshape(group_tokens, 128),
                (((0,), (0,)), ((), ())), precision=lax.Precision.HIGHEST,
                preferred_element_type=F32,
            )
            for g in range(groups)
        ],
        axis=0,
    )[:, :1]
    for y in far_lines:
        gate, up = expert_in(same_core(y), gate, up)
    for y in far_lines:
        for k in range(groups):
            arrived_g(k, group_from[k], other_core(y))
        gate, up = expert_in(other_core(y), gate, up)
    expert_hidden = (silu(gate * slot_scale) * (up * slot_scale)).astype(BF)
    returns = far_groups + [my_group]

    def near_e(k):
        g = returns[k]
        return tp_copy(e_part.at[1 - core, g], e_near.at[g], "e1", sibling, k)

    def far_e(k, y):
        g = returns[k]
        return tp_copy(e_send.at[g, y], e_recv.at[g, line], "e2", same_core(y), k)

    def expert_out(which, y):
        part = dot(expert_hidden, w_ed[0, :, columns_of(2 * y + which)])
        e_part[which, :, y] = part.reshape(groups, group_slots, chunk).astype(BF)

    for y in range(lines):
        expert_out(1 - core, y)
    for k in range(groups):
        near_e(k).start()
    for y in range(lines):
        expert_out(core, y)
    for k in range(groups):
        g = returns[k]
        near_e(k).wait_recv()
        for y in far_lines:
            e_send[g, y] = (e_part[core, g, y].astype(F32) + e_near[g, y].astype(F32)).astype(BF)
            far_e(k, y).start()
    drains.append(tp_copy(e_part.at[0], e_near, "e1", sibling))
    other_lines = pl.ds(0, lines - 1)
    sent = e_send.at[pl.ds(0, groups), other_lines]
    drains.append(tp_copy(sent, e_recv.at[pl.ds(0, groups), other_lines], "e2", sibling))
    pre = d_half[0]
    for y in far_lines:
        tp_copy(d_send.at[0], d_far.at[y], "d2", same_core(y), y).wait_recv()
        pre = pre + d_far[y].astype(F32)
    half_blocks = n_ep // 2
    pre = pre * scale_ref[pl.ds(core * half_blocks, half_blocks)].reshape(half_rows, 128)[:, :1]
    h_all[core] = (silu(pre[:, :hidden]) * pre[:, hidden:]).astype(BF)
    sent_h = tp_copy(h_all.at[core], h_all.at[core], "h", sibling)
    sent_h.start()
    drains.append(sent_h)
    tp_copy(h_all.at[core], h_all.at[1 - core], "h", sibling).wait_recv()
    dense_hidden = h_all[...].astype(F32).reshape(batch, hidden).astype(BF)
    dense = dot(dense_hidden, w_dd[...]) * (1.0 / (1.0 + jnp.exp(-mix[...])))
    dense_ref[...] = dense.reshape(n_ep, rows, chunk)

    def near_f(k):
        g = returns[k]
        return ep_copy(f_away.at[g], f_mate.at[g], "f1", mate, k)

    def far_f(k):
        g = returns[k]
        near_f(k).wait_recv()
        both = comb[g, par] + f_mate[g].astype(F32)
        comb[g, par] = both
        f_send[pl.ds(g * group_pairs, group_pairs)] = both.astype(BF)
        for q in pairs_in(g, k == groups - 1):
            ep_copy(f_send.at[q], f_recv.at[pair], "f2", twin(q), pair).start()

    for k in range(groups):
        g = returns[k]
        block = pl.ds(g * members, members)
        result = e_part[core, g, line].astype(F32) + e_near[g, line].astype(F32)
        tp_copy(e_send.at[g, other_lines], e_recv.at[g, other_lines], "e2", sibling, k).wait_recv()
        for y in far_lines:
            result = result + e_recv[g, y].astype(F32)
        coef = c_recv[block].reshape(group_tokens, 128)[:, :1]
        mixed = coef * dot(place_ref[g], result.astype(BF))
        combined = dense_ref[block] + mixed.reshape(members, rows, chunk)
        for m in range(members):
            comb[g, m % 2, m // 2] = combined[m]
        f_away[g] = comb[g, 1 - par].astype(BF)
        near_f(k).start()
        if k > 0:
            far_f(k - 1)
    far_f(groups - 1)
    drains.append(ep_copy(f_away, f_mate, "f1", mate))
    drains.append(ep_copy(f_send.at[far_blocks], f_recv.at[far_blocks], "f2", mate))
    final = middle_ref[...] + comb[my_group, par, lax.rem(pair, group_pairs)]
    for q in others:
        ep_copy(f_send.at[q], f_recv.at[q], "f2", twin(q), q).wait_recv()
        final = final + f_recv[q].astype(F32)
    out[...] = final.astype(BF)
    for copy in drains:
        copy.wait_send()


def per_device(
    tokens, delta_state, attn_gain, query_weight, key_weight, value_weight, decay_weight,
    beta_weight, decay_rate, head_gain, output_weight, ffn_gain, expert_ids, group_prob,
    expert_logit, expert_gate, expert_up, expert_down, dense_gate, dense_up, dense_down, dense_mix,
):
    n_ep = lax.axis_size("ep")
    n_tp = lax.axis_size("tp")
    rows, width = tokens.shape
    heads = delta_state.shape[1]
    local = heads * 128
    topk = expert_ids.shape[1]
    cap = max(2, 2 * rows * topk // n_ep)
    members = max(2, 8 // math.gcd(cap, 8))
    if n_ep % members:
        members = n_ep
    groups = n_ep // members
    group_slots = members * cap
    chunk = width // n_tp
    depth = width // n_ep
    batch = n_ep * rows
    pairs = n_ep // 2
    lines = n_tp // 2
    hidden = dense_gate.shape[1]
    small = (
        tokens, attn_gain[None, :], decay_rate[None, :], head_gain[None, :], ffn_gain[None, :],
        expert_ids.T, group_prob[None, :], expert_logit.T, dense_mix[None, :],
    )
    weights = (
        delta_state, decay_weight.T, beta_weight.T, query_weight, key_weight, value_weight,
        output_weight, dense_gate, dense_up, expert_gate, expert_up, expert_down, dense_down,
    )
    arrays = tuple(pltpu.with_memory_space_constraint(a, pltpu.HBM) for a in small + weights)
    starts, n_sems = semaphores(n_ep, n_tp, groups, len(arrays))
    dims = (n_ep, n_tp, rows, width, heads, members, cap, len(arrays), starts)
    vmem = pl.BlockSpec(memory_space=pltpu.VMEM)
    kq_rows = -(-2 * heads // 8) * 8
    scratch = [pltpu.VMEM(a.shape, a.dtype) for a in small + weights[1:]]
    scratch += [
        pltpu.VMEM(shape, dtype)
        for shape, dtype in (
            ((n_ep, rows, depth), BF), ((n_ep, rows, depth), BF),
            ((3, pairs, rows, local), BF), ((3, pairs, rows, local), BF),
            ((3, pairs, rows, local), F32),
            ((3, pairs, rows, local), BF), ((3, pairs, rows, local), BF),
            ((n_ep, 8, 128), F32), ((n_ep, 8, 128), F32), ((n_ep, rows, 128), F32),
            ((rows, kq_rows, 128), F32), ((2 * heads, rows, 128), F32),
            ((heads, rows, 128), F32), ((heads, rows, 128), F32), ((rows, local), BF),
            ((n_tp, rows, chunk), BF), ((n_tp, rows, chunk), BF), ((n_tp, rows, 128), F32),
            ((n_ep, 8, 128), F32), ((n_ep, rows, 128), F32), ((rows, chunk), F32),
            ((n_ep, rows, chunk), BF), ((n_tp, groups, group_slots, chunk), BF),
            ((2, batch // 2, 2 * hidden), F32), ((2, batch // 2, 2 * hidden), BF),
            ((batch // 2, 2 * hidden), BF), ((lines, batch // 2, 2 * hidden), BF),
            ((2, batch // 2, hidden), BF),
            ((2, groups, lines, group_slots, chunk), BF), ((groups, lines, group_slots, chunk), BF),
            ((groups, lines, group_slots, chunk), BF), ((groups, lines, group_slots, chunk), BF),
            ((groups, 2, members // 2, rows, chunk), F32),
            ((groups, members // 2, rows, chunk), BF), ((groups, members // 2, rows, chunk), BF),
            ((pairs, rows, chunk), BF), ((pairs, rows, chunk), BF),
            ((groups, members * rows, group_slots), BF), ((n_ep, rows, chunk), F32),
        )
    ]
    scratch += [pltpu.SemaphoreType.DMA((n_sems,))]
    mixed_out, new_state = pl.pallas_call(
        functools.partial(kernel, dims),
        out_shape=(pltpu.VMEM((rows, chunk), BF), pltpu.VMEM(delta_state.shape, F32)),
        in_specs=[pl.BlockSpec(memory_space=pltpu.HBM)] * len(arrays),
        out_specs=(vmem, vmem),
        scratch_shapes=scratch,
        compiler_params=pltpu.CompilerParams(
            collective_id=0, has_side_effects=True, vmem_limit_bytes=44 * 1024 * 1024
        ),
    )(*arrays)
    new_state, mixed_out = pl.pallas_call(
        store_kernel,
        out_shape=(pltpu.HBM(delta_state.shape, F32), pltpu.HBM((rows, chunk), BF)),
        in_specs=[vmem] * 2,
        out_specs=(pl.BlockSpec(memory_space=pltpu.HBM),) * 2,
        scratch_shapes=[pltpu.SemaphoreType.DMA((rows + 1,))],
        compiler_params=pltpu.CompilerParams(vmem_limit_bytes=8 * 1024 * 1024),
    )(*(pltpu.with_memory_space_constraint(a, pltpu.VMEM) for a in (new_state, mixed_out)))
    return mixed_out, new_state


def solution(mesh):
    return jax.shard_map(
        per_device,
        mesh=mesh,
        in_specs=(
            P("ep", None), P("ep", "tp", None, None), P(), P("ep", "tp"), P("ep", "tp"),
            P("ep", "tp"), P(), P(), P("tp"), P(), P("tp", None), P(), P("ep", None), P("ep"),
            P("ep", None), P("ep", None, "tp"), P("ep", None, "tp"), P("ep", "tp", None),
            P("tp", "ep"), P("tp", "ep"), P("ep", "tp"), P("tp"),
        ),
        out_specs=(P("ep", "tp"), P("ep", "tp", None, None)),
        check_vma=False,
    )
```

time: 69.7 us -> 64.4 us (0.924)
  local copies, waits for them, and re-layouts: 3.33 us -> 0 us
  Pallas kernels: 65.6 us -> 63.6 us
    unnamed x2 -> x0, local copies, waits for them, and re-layouts: 3.33 us -> none
    pallas_call x1 -> x2, Pallas kernels: 65.6 us -> 63.6 us  [the longest x1 60.7 us: per_device(): pl.pallas_call(functools.partial(kernel, dims), out_shape=(pltpu.VMEM((ro...]
where the time goes in v3:
time: 64.4 us; the launch traced here: 64.2 us
  Pallas kernels  63.6 us (99%)
  between operations  0.65 us (1%)
    pallas_call x1, Pallas kernels, per_device(): pl.pallas_call(functools.partial(kernel, dims), out_shape=(pltpu.VMEM((ro...  60.7 us
    pallas_call x1, Pallas kernels, per_device(): pl.pallas_call(store_kernel, out_shape=(pltpu.HBM(delta_state.shape, F32)...  2.87 us

profile of v3, /device:TPU:0, one launch (start us, length us, event | category | flops | bytes accessed | tf_op | source)
XLA Modules:
  0.0 64.2 jit_solution(1111004421674077622)
XLA Ops:
  0.6 60.7 %shard_map.221 = (bf16[24,1024]{1,0:T(8,128)(2,1)S(1)}, f32[24,4,128,128]{3,2,1,0:T(8,128)S(1)}) custom-call(bf16[24,4096]{1,0:T(8,128)(2,1)} %refs_0_.1, f32[1,4096]{1,0:T(1,128)} %bitcast.12, f32[1,4]{1,0:T(1,128)} %bitcast.17, f32[1,128]{1,0:T(1,128)} %bitcast.18, f32[1,4096]{1,0:T(1,128)} %bitcast.13, s32[2,24]{1,0:T(2,128)} %bitcast.15, ...), custom_call_target="tpu_custom_call" | custom-call | tf_op jit(solution)/shard_map/pallas_call | solution.py:596
  61.4 2.9 %shard_map.222 = (f32[24,4,128,128]{3,2,1,0:T(8,128)}, bf16[24,1024]{1,0:T(8,128)(2,1)}) custom-call(f32[24,4,128,128]{3,2,1,0:T(8,128)S(1)} %get-tuple-element.6.state, bf16[24,1024]{1,0:T(8,128)(2,1)S(1)} %get-tuple-element.7.mixed), custom_call_target="tpu_custom_call" | custom-call | tf_op jit(solution)/shard_map/pallas_call | solution.py:606

commit v4 on v3

--- a/solution.py
+++ b/solution.py
@@ -9,6 +9,13 @@
 from jax.sharding import PartitionSpec as P
 
 EPS = 1e-06
+CROSS_AT = 2
+RECALL = 4
+UPDATE = 4
+X_STRAIGHT = (2,)
+F_STRAIGHT = (0, 2)
+X_SENDS = (0, 1, 2)
+X_ORDER = (2, 0, 1)
 BF = jnp.bfloat16
 F32 = jnp.float32
 MESH = pl.DeviceIdType.MESH
@@ -37,25 +44,36 @@
     return order
 
 
+def partners(position, count):
+    if count == 4:
+        low, high = lax.rem(position, 2), lax.div(position, 2)
+        return [3 - position, position + 2 - 4 * high, position + 1 - 2 * low]
+    return far_first(position, count)
+
+
 def store_kernel(state, mixed, state_out, mixed_out, sems):
     rows = state.shape[0]
-    copies = [pltpu.make_async_copy(mixed, mixed_out, sems.at[rows])]
-    copies += [
-        pltpu.make_async_copy(state.at[r], state_out.at[r], sems.at[r]) for r in range(rows)
-    ]
-    for copy in copies:
-        copy.start()
-    for copy in copies:
-        copy.wait()
-
-
-def semaphores(n_ep, n_tp, groups, n_in):
+    small = pltpu.make_async_copy(mixed, mixed_out, sems.at[1])
+    small.start()
+    for r in range(rows):
+        pltpu.make_async_copy(state.at[r], state_out.at[r], sems.at[0]).start()
+    pltpu.make_async_copy(state, state_out, sems.at[0]).wait()
+    small.wait()
+
+
+def dense_steps(groups):
+    return 1 if groups % 2 else groups // 2
+
+
+def semaphores(n_ep, n_tp, members, n_in):
+    groups = n_ep // members
     pairs, lines = n_ep // 2, n_tp // 2
+    steps = dense_steps(groups)
     sizes = {
-        "load": n_in, "ns": 1, "nr": 1, "cs": 1, "cr": 1, "zs": 1, "zr": 1,
-        "q1s": 1, "q1r": 3, "q2s": 1, "q2r": 3, "xs": 1, "xr": n_ep,
-        "f1s": 1, "f1r": groups, "f2s": 1, "f2r": pairs, "as": 1, "ar": 1, "ss": 1, "sr": 1,
-        "d1s": 1, "d1r": 1, "d2s": 1, "d2r": lines, "hs": 1, "hr": 1,
+        "load": n_in, "ns": 1, "nr": pairs + 1, "ms": 1, "mr": 1, "cs": 1, "cr": 1, "zs": 1, "zr": 1,
+        "q1s": 1, "q1r": 2, "q2s": 1, "q2r": 2, "k1s": 1, "k1r": 1, "k2s": 1, "k2r": 1, "xs": 1, "xr": n_ep,
+        "f1s": 1, "f1r": groups, "f2s": 1, "f2r": n_ep, "as": 1, "ar": 1, "ss": 1, "sr": 1,
+        "d1s": 1, "d1r": steps, "d2s": 1, "d2r": steps * lines, "hs": 1, "hr": steps,
         "gs": 1, "gr": groups * n_tp, "e1s": 1, "e1r": groups, "e2s": 1, "e2r": groups,
     }
     starts, total = {}, 0
@@ -74,7 +92,7 @@
     (tokens, attn_gain, decay_rate, head_gain, ffn_gain, ids, group_prob, logit, mix) = held[:9]
     state, w_decay, w_beta, w_q, w_k, w_v, w_o, w_dg, w_du, w_eg, w_eu, w_ed, w_dd = held[9:]
     (
-        n_send, n_recv, q_away, q_mate, q_own, q_send, q_recv, c_send, c_rows, c_recv, kq, recall,
+        n_send, n_recv, k_own, k_send, k_recv, k_away, k_mate, q_away, q_mate, q_own, q_send, q_recv, c_send, c_rows, c_recv, kq, recall,
         corr_ref, decay_ref, head_out, a_send, a_recv, s_recv, scale_rows, scale_ref, middle_ref,
         x_all, g_all, d_half, d_send, d_near, d_far, h_all, e_part, e_near, e_send, e_recv,
         comb, f_away, f_mate, f_send, f_recv, place_ref, dense_ref, sems,
@@ -99,7 +117,11 @@
     line = lax.div(my, 2)
     sibling = my + 1 - 2 * core
     my_group = lax.div(pair, group_pairs)
-    far_groups = far_first(my_group, groups)
+    far_groups = partners(my_group, groups)
+    x_straight = {4: X_STRAIGHT, 2: (0,)}.get(groups, ())
+    f_straight = {4: F_STRAIGHT, 2: (0,)}.get(groups, ())
+    x_sends = X_SENDS if groups == 4 else range(groups - 1)
+    x_order = X_ORDER if groups == 4 else range(groups - 1)
     far_lines = [lax.rem(line + d, lines) for d in range(1, lines)]
 
     def same_core(y):
@@ -167,10 +189,16 @@
     for p in range(n_ep):
         n_send[p] = normed[:, p * depth : (p + 1) * depth]
     pl.semaphore_wait(barrier, n_ep + n_tp - 2)
-    here = par * pairs + pair
-    for p in ep_peers:
-        ep_copy(n_send.at[p], n_recv.at[here], "n", p).start()
-    n_recv[here] = n_send[me]
+    def shelf(p):
+        return lax.rem(p, 2) * pairs + lax.div(p, 2)
+
+    def carried(q):
+        return 2 * q + lax.rem(par + pair + q + core, 2)
+
+    for q in others:
+        ep_copy(n_send.at[carried(q)], n_recv.at[shelf(me)], "n", carried(q), pair).start()
+    ep_copy(n_send.at[mate], n_recv.at[shelf(me)], "n", mate, pairs).start()
+    n_recv[shelf(me)] = n_send[me]
 
     logit_exp = jnp.exp(logit[...])
     route = group_prob[...] * logit_exp / jnp.sum(logit_exp, axis=0, keepdims=True)
@@ -206,21 +234,34 @@
         loads[i].wait()
 
     most = pl.ds(0, n_ep - 1)
-    done_n = ep_copy(n_send.at[most], n_recv.at[most], "n", mate)
-    done_n.wait_recv()
-    drains.append(done_n)
+    some = pl.ds(0, pairs - 1)
+    for q in others:
+        block = n_recv.at[shelf(carried(q))]
+        ep_copy(block, block, "n", mate, q).wait_recv()
+        tp_copy(block, block, "m", sibling).start()
+    ep_copy(n_send.at[mate], n_recv.at[shelf(mate)], "n", mate, pairs).wait_recv()
+    drains.append(ep_copy(n_send.at[pl.ds(0, pairs)], n_recv.at[pl.ds(0, pairs)], "n", mate))
+    passed = tp_copy(n_recv.at[some], n_recv.at[some], "m", sibling)
+    passed.wait_recv()
+    drains.append(passed)
 
     def rows_of(parity):
         held_rows = n_recv[pl.ds(parity * pairs, pairs)].astype(F32)
         return held_rows.reshape(pairs * rows, depth).astype(BF)
 
     away, near = rows_of(1 - par), rows_of(par)
-    for j, w in enumerate((w_k, w_q, w_v)):
+    k_part = dot(jnp.concatenate([away, near], axis=0), w_k[...]).reshape(2, pairs, rows, local)
+    k_own[...] = k_part
+    for side in range(2):
+        k_send[:, side] = k_part[side].astype(BF)
+    for q in others:
+        ep_copy(k_send.at[q], k_recv.at[pair], "k1", twin(q)).start()
+    for j, w in enumerate((w_q, w_v)):
         q_away[j] = dot(away, w[...]).reshape(pairs, rows, local).astype(BF)
         ep_copy(q_away.at[j], q_mate.at[j], "q1", mate, j).start()
-    for j, w in enumerate((w_k, w_q, w_v)):
+    for j, w in enumerate((w_q, w_v)):
         q_own[j] = dot(near, w[...]).reshape(pairs, rows, local)
-    for j in range(3):
+    for j in range(2):
         ep_copy(q_away.at[j], q_mate.at[j], "q1", mate, j).wait_recv()
         both = q_own[j] + q_mate[j].astype(F32)
         q_own[j] = both
@@ -229,8 +270,22 @@
             ep_copy(q_send.at[j, q], q_recv.at[j, pair], "q2", twin(q), j).start()
     drains.append(ep_copy(q_away, q_mate, "q1", mate))
     far_blocks = pl.ds(0, pairs - 1)
-    sent = q_send.at[pl.ds(0, 3), far_blocks]
-    drains.append(ep_copy(sent, q_recv.at[pl.ds(0, 3), far_blocks], "q2", mate))
+    sent = q_send.at[pl.ds(0, 2), far_blocks]
+    drains.append(ep_copy(sent, q_recv.at[pl.ds(0, 2), far_blocks], "q2", mate))
+    done_k = ep_copy(k_send.at[far_blocks], k_recv.at[far_blocks], "k1", mate)
+    done_k.wait_recv()
+    drains.append(done_k)
+    sums = []
+    for side in range(2):
+        total = k_own[side, pair]
+        for q in others:
+            total = total + k_recv[q, side].astype(F32)
+        sums.append(total)
+        if side == 0:
+            k_away[...] = total.astype(BF)
+            cross_k = ep_copy(k_away, k_mate, "k2", mate)
+            cross_k.start()
+            drains.append(cross_k)
 
     def summed(j):
         ep_copy(
@@ -241,8 +296,9 @@
             total = total + q_recv[j, q].astype(F32)
         return total.astype(BF).astype(F32)
 
-    k_rows = summed(0)
-    q_rows = summed(1)
+    q_rows = summed(0)
+    cross_k.wait_recv()
+    k_rows = (sums[1] + k_mate[...].astype(F32)).astype(BF).astype(F32)
     loads[state_i].wait()
 
     def head_of(values, h):
@@ -259,16 +315,21 @@
         kq[:, h, :] = k_unit
         kq[:, heads + h, :] = q_unit
 
+    beside = 2 if heads % 2 == 0 else 1
+
     def one_row(b, _):
         both = kq[b].astype(BF)
-        for h in range(heads):
-            read = dot(both, state[b, h].astype(BF))
-            recall[h, pl.ds(b, 1), :] = read[h : h + 1]
-            recall[heads + h, pl.ds(b, 1), :] = read[heads + h : heads + h + 1]
+        for first in range(0, heads, beside):
+            pieces = [state[b, first + i].astype(BF) for i in range(beside)]
+            read = dot(both, jnp.concatenate(pieces, axis=1))
+            for i in range(beside):
+                h, lanes = first + i, slice(i * 128, (i + 1) * 128)
+                recall[h, pl.ds(b, 1), :] = read[h : h + 1, lanes]
+                recall[heads + h, pl.ds(b, 1), :] = read[heads + h : heads + h + 1, lanes]
         return 0
 
-    lax.fori_loop(0, rows, one_row, 0, unroll=4)
-    v_rows = summed(2)
+    lax.fori_loop(0, rows, one_row, 0, unroll=RECALL)
+    v_rows = summed(1)
     for h in range(heads):
         q_unit, k_unit = units[h]
         decay, beta = decays[h], betas[h]
@@ -299,7 +360,7 @@
             state[b, h] = decay * state[b, h] + columns[:, h : h + 1] * corr
         return 0
 
-    lax.fori_loop(0, rows // 2, update_row, 0, unroll=4)
+    lax.fori_loop(0, rows // 2, update_row, 0, unroll=UPDATE)
     middle = tokens[:, own].astype(F32)
     most_tp = pl.ds(0, n_tp - 1)
     done_a = tp_copy(a_send.at[most_tp], a_recv.at[most_tp], "a", sibling)
@@ -308,13 +369,18 @@
     for p in range(n_tp):
         middle = middle + a_recv[p].astype(F32)
     x_all[me] = (middle * ffn_gain[:, own]).astype(BF)
-    for p in [mate] + [twin(q) for q in others]:
+    x_peers = [mate] + [twin(q) for q in pairs_in(my_group, True)]
+    for i in x_sends:
+        x_peers += [twin(q) for q in pairs_in(far_groups[i])]
+        if i in x_straight:
+            x_peers += [cross(q) for q in pairs_in(far_groups[i])]
+    for p in x_peers:
         ep_copy(x_all.at[me], x_all.at[me], "x", p, me).start()
     middle_ref[...] = middle
     s_recv[my] = jnp.broadcast_to(jnp.sum(middle * middle, axis=-1, keepdims=True), (rows, 128))
     for p in tp_peers:
         tp_copy(s_recv.at[my], s_recv.at[my], "s", p).start()
-    lax.fori_loop(rows // 2, rows, update_row, 0, unroll=4)
+    lax.fori_loop(rows // 2, rows, update_row, 0, unroll=UPDATE)
     done_c = ep_copy(c_send.at[most], c_rows.at[most], "c", mate)
     done_c.wait_recv()
     drains.append(done_c)
@@ -349,7 +415,7 @@
 
     def send_g(k, g):
         block = g_all.at[my, g]
-        for p in [same_core(y) for y in far_lines] + [sibling]:
+        for p in [sibling] + [same_core(y) for y in far_lines]:
             tp_copy(block, block, "g", p, k * n_tp + my).start()
 
     def pass_on(k, g):
@@ -363,18 +429,79 @@
         block = g_all.at[p, g]
         tp_copy(block, block, "g", p, k * n_tp + p).wait_recv()
 
-    def forward_x(g, own_group):
-        for q in pairs_in(g, own_group):
+    def forward_x(k):
+        for q in pairs_in(group_from[k], k == 0):
             block = x_all.at[twin(q)]
             ep_copy(block, block, "x", twin(q), twin(q)).wait_recv()
             ep_copy(block, block, "x", mate, twin(q)).start()
 
-    group_from = [my_group] + far_groups
-    forward_x(my_group, True)
+    group_from = [my_group] + [far_groups[i] for i in x_order]
+    hidden = w_dg.shape[1]
+    if groups % 2:
+        units = [(u * pairs, pairs) for u in range(2)]
+    else:
+        units = [(g * members, members) for g in group_from]
+    steps = len(units) // 2
+    unit_rows = units[0][1] * rows
+    loads[dg_i].wait()
+    loads[du_i].wait()
+
+    def unit_of(ref, u):
+        start, count = units[u]
+        return ref.at[pl.ds(start, count)]
+
+    def near_d(h):
+        return tp_copy(d_send.at[h, 1], d_near.at[h], "d1", sibling, h)
+
+    def far_d(h, y, source):
+        return tp_copy(d_send.at[h, 0], d_far.at[h, source], "d2", same_core(y), h * lines + source)
+
+    def dense_dots(h):
+        xs = jnp.concatenate(
+            [
+                unit_of(x_all, 2 * h + u)[...].astype(F32).reshape(unit_rows, chunk)
+                for u in range(2)
+            ],
+            axis=0,
+        ).astype(BF)
+        for j, w in enumerate((w_dg, w_du)):
+            part = dot(xs, w[...]).reshape(2, unit_rows, hidden)
+            d_half[h, :, :, j * hidden : (j + 1) * hidden] = part
+        d_send[h, 1] = d_half[h, 1 - core].astype(BF)
+        near_d(h).start()
+
+    def dense_cross(h):
+        near_d(h).wait_recv()
+        pre = d_half[h, core] + d_near[h].astype(F32)
+        d_half[h, 0] = pre
+        d_send[h, 0] = pre.astype(BF)
+        for y in far_lines:
+            far_d(h, y, line).start()
+
+    def dense_hide(h):
+        pre = d_half[h, 0]
+        for y in far_lines:
+            far_d(h, y, y).wait_recv()
+            pre = pre + d_far[h, y].astype(F32)
+        first, count = units[2 * h][0] * (1 - core) + units[2 * h + 1][0] * core, units[2 * h][1]
+        pre = pre * scale_ref[pl.ds(first, count)].reshape(unit_rows, 128)[:, :1]
+        h_all[2 * h + core] = (silu(pre[:, :hidden]) * pre[:, hidden:]).astype(BF)
+        sent_h(h).start()
+
+    def sent_h(h):
+        return tp_copy(h_all.at[2 * h + core], h_all.at[2 * h + core], "h", sibling, h)
+
+    forward_x(0)
+    relayed = [k + 1 for k, i in enumerate(x_order) if i not in x_straight]
     for k in range(groups):
         g = group_from[k]
-        if k + 1 < groups:
-            forward_x(group_from[k + 1], False)
+        if k < len(relayed):
+            forward_x(relayed[k])
+        if steps == 2 and k == CROSS_AT:
+            dense_cross(0)
+        if k > 0 and k not in relayed:
+            for q in pairs_in(g):
+                ep_copy(x_all.at[me], x_all.at[twin(q)], "x", mate, twin(q)).wait_recv()
         for q in pairs_in(g, k == 0) + ([pair] if k == 0 else []):
             ep_copy(x_all.at[me], x_all.at[cross(q)], "x", mate, cross(q)).wait_recv()
         block = x_all[pl.ds(g * members, members)].astype(F32)
@@ -385,21 +512,18 @@
         send_g(k, g)
         if k > 1:
             pass_on(k - 2, group_from[k - 2])
+        if steps == 2 and k == 1:
+            dense_dots(0)
     drains.append(ep_copy(x_all.at[most], x_all.at[most], "x", mate))
     drains.append(tp_copy(g_all.at[most_tp], g_all.at[most_tp], "g", sibling))
-    for i in (dg_i, du_i, eg_i, eu_i, ed_i, dd_i):
+    for i in (eg_i, eu_i, ed_i, dd_i):
         loads[i].wait()
-    xs = x_all[...].astype(F32).reshape(batch, chunk).astype(BF)
-    hidden = w_dg.shape[1]
-    half_rows = batch // 2
-    for j, w in enumerate((w_dg, w_du)):
-        d_half[:, :, j * hidden : (j + 1) * hidden] = dot(xs, w[...]).reshape(2, half_rows, hidden)
-    d_send[1] = d_half[1 - core].astype(BF)
-    near_d = tp_copy(d_send.at[1], d_near, "d1", sibling)
-    near_d.start()
-    drains.append(near_d)
+    for h in range(0 if steps != 2 else 1, steps):
+        dense_dots(h)
     if groups > 1:
         pass_on(groups - 2, group_from[groups - 2])
+    if steps == 2 and CROSS_AT == 4:
+        dense_cross(0)
 
     def expert_in(p, gate, up):
         routed = g_all[p].astype(F32).reshape(slots, chunk).astype(BF)
@@ -409,18 +533,12 @@
 
     gate = jnp.zeros((slots, w_eg.shape[2]), F32)
     gate, up = expert_in(my, gate, gate)
+    pass_on(groups - 1, group_from[groups - 1])
     for k in range(groups):
         arrived_g(k, group_from[k], sibling)
     gate, up = expert_in(sibling, gate, up)
-    near_d.wait_recv()
-    pre = d_half[core] + d_near[...].astype(F32)
-    d_half[0] = pre
-    d_send[0] = pre.astype(BF)
-    for y in far_lines:
-        tp_copy(d_send.at[0], d_far.at[line], "d2", same_core(y), line).start()
-    for y in far_lines:
-        drains.append(tp_copy(d_send.at[0], d_far.at[line], "d2", same_core(y), line))
-    pass_on(groups - 1, group_from[groups - 1])
+    for h in range(0 if steps != 2 else 1, steps):
+        dense_cross(h)
     done_z = ep_copy(scale_rows.at[most], scale_rows.at[most], "z", mate)
     done_z.wait_recv()
     drains.append(done_z)
@@ -438,6 +556,8 @@
         ],
         axis=0,
     )[:, :1]
+    for h in range(steps - 1):
+        dense_hide(h)
     for y in far_lines:
         gate, up = expert_in(same_core(y), gate, up)
     for y in far_lines:
@@ -475,20 +595,20 @@
     other_lines = pl.ds(0, lines - 1)
     sent = e_send.at[pl.ds(0, groups), other_lines]
     drains.append(tp_copy(sent, e_recv.at[pl.ds(0, groups), other_lines], "e2", sibling))
-    pre = d_half[0]
+    dense_hide(steps - 1)
+    for h in range(steps):
+        tp_copy(h_all.at[core], h_all.at[2 * h + 1 - core], "h", sibling, h).wait_recv()
+    drains.append(tp_copy(h_all.at[pl.ds(0, steps)], h_all.at[pl.ds(0, steps)], "h", sibling))
+    sent = d_send.at[pl.ds(0, steps), 1]
+    drains.append(tp_copy(sent, d_near, "d1", sibling))
     for y in far_lines:
-        tp_copy(d_send.at[0], d_far.at[y], "d2", same_core(y), y).wait_recv()
-        pre = pre + d_far[y].astype(F32)
-    half_blocks = n_ep // 2
-    pre = pre * scale_ref[pl.ds(core * half_blocks, half_blocks)].reshape(half_rows, 128)[:, :1]
-    h_all[core] = (silu(pre[:, :hidden]) * pre[:, hidden:]).astype(BF)
-    sent_h = tp_copy(h_all.at[core], h_all.at[core], "h", sibling)
-    sent_h.start()
-    drains.append(sent_h)
-    tp_copy(h_all.at[core], h_all.at[1 - core], "h", sibling).wait_recv()
+        sent = d_send.at[pl.ds(0, steps), 0]
+        drains.append(tp_copy(sent, d_far.at[pl.ds(0, steps), line], "d2", same_core(y)))
     dense_hidden = h_all[...].astype(F32).reshape(batch, hidden).astype(BF)
     dense = dot(dense_hidden, w_dd[...]) * (1.0 / (1.0 + jnp.exp(-mix[...])))
-    dense_ref[...] = dense.reshape(n_ep, rows, chunk)
+    for u in range(len(units)):
+        part = dense[u * unit_rows : (u + 1) * unit_rows]
+        unit_of(dense_ref, u)[...] = part.reshape(units[u][1], rows, chunk)
 
     def near_f(k):
         g = returns[k]
@@ -499,9 +619,21 @@
         near_f(k).wait_recv()
         both = comb[g, par] + f_mate[g].astype(F32)
         comb[g, par] = both
-        f_send[pl.ds(g * group_pairs, group_pairs)] = both.astype(BF)
-        for q in pairs_in(g, k == groups - 1):
+        send_f(g, both, k == groups - 1)
+
+    def send_f(g, values, own_group):
+        f_send[pl.ds(g * group_pairs, group_pairs)] = values.astype(BF)
+        for q in pairs_in(g, own_group):
             ep_copy(f_send.at[q], f_recv.at[pair], "f2", twin(q), pair).start()
+
+    def straight_f(k, g):
+        send_f(g, comb[g, par], False)
+        first = pairs + f_straight.index(k) * group_pairs
+        f_send[pl.ds(first, group_pairs)] = comb[g, 1 - par].astype(BF)
+        for m in range(group_pairs):
+            spare = first + lax.rem(pair, group_pairs)
+            q = g * group_pairs + m
+            ep_copy(f_send.at[first + m], f_recv.at[spare], "f2", cross(q), spare).start()
 
     for k in range(groups):
         g = returns[k]
@@ -515,16 +647,24 @@
         combined = dense_ref[block] + mixed.reshape(members, rows, chunk)
         for m in range(members):
             comb[g, m % 2, m // 2] = combined[m]
-        f_away[g] = comb[g, 1 - par].astype(BF)
-        near_f(k).start()
-        if k > 0:
-            far_f(k - 1)
-    far_f(groups - 1)
-    drains.append(ep_copy(f_away, f_mate, "f1", mate))
-    drains.append(ep_copy(f_send.at[far_blocks], f_recv.at[far_blocks], "f2", mate))
+        if k in f_straight:
+            straight_f(k, g)
+        else:
+            f_away[g] = comb[g, 1 - par].astype(BF)
+            near_f(k).start()
+        if k > 1 and k - 2 not in f_straight:
+            far_f(k - 2)
+    for k in range(max(0, groups - 2), groups):
+        if k not in f_straight:
+            far_f(k)
+    met = pl.ds(0, groups - len(f_straight))
+    drains.append(ep_copy(f_away.at[met], f_mate.at[met], "f1", mate))
+    spares = list(range(pairs, pairs + len(f_straight) * group_pairs))
+    sent = pl.ds(0, pairs - 1 + len(spares))
+    drains.append(ep_copy(f_send.at[sent], f_recv.at[sent], "f2", mate))
     final = middle_ref[...] + comb[my_group, par, lax.rem(pair, group_pairs)]
-    for q in others:
-        ep_copy(f_send.at[q], f_recv.at[q], "f2", twin(q), q).wait_recv()
+    for q in others + spares:
+        ep_copy(f_send.at[q], f_recv.at[q], "f2", mate, q).wait_recv()
         final = final + f_recv[q].astype(F32)
     out[...] = final.astype(BF)
     for copy in drains:
@@ -563,7 +703,9 @@
         output_weight, dense_gate, dense_up, expert_gate, expert_up, expert_down, dense_down,
     )
     arrays = tuple(pltpu.with_memory_space_constraint(a, pltpu.HBM) for a in small + weights)
-    starts, n_sems = semaphores(n_ep, n_tp, groups, len(arrays))
+    steps = dense_steps(groups)
+    unit_rows = batch // (2 * steps)
+    starts, n_sems = semaphores(n_ep, n_tp, members, len(arrays))
     dims = (n_ep, n_tp, rows, width, heads, members, cap, len(arrays), starts)
     vmem = pl.BlockSpec(memory_space=pltpu.VMEM)
     kq_rows = -(-2 * heads // 8) * 8
@@ -572,23 +714,25 @@
         pltpu.VMEM(shape, dtype)
         for shape, dtype in (
             ((n_ep, rows, depth), BF), ((n_ep, rows, depth), BF),
-            ((3, pairs, rows, local), BF), ((3, pairs, rows, local), BF),
-            ((3, pairs, rows, local), F32),
-            ((3, pairs, rows, local), BF), ((3, pairs, rows, local), BF),
+            ((2, pairs, rows, local), F32), ((pairs, 2, rows, local), BF),
+            ((pairs, 2, rows, local), BF), ((rows, local), BF), ((rows, local), BF),
+            ((2, pairs, rows, local), BF), ((2, pairs, rows, local), BF),
+            ((2, pairs, rows, local), F32),
+            ((2, pairs, rows, local), BF), ((2, pairs, rows, local), BF),
             ((n_ep, 8, 128), F32), ((n_ep, 8, 128), F32), ((n_ep, rows, 128), F32),
             ((rows, kq_rows, 128), F32), ((2 * heads, rows, 128), F32),
             ((heads, rows, 128), F32), ((heads, rows, 128), F32), ((rows, local), BF),
             ((n_tp, rows, chunk), BF), ((n_tp, rows, chunk), BF), ((n_tp, rows, 128), F32),
             ((n_ep, 8, 128), F32), ((n_ep, rows, 128), F32), ((rows, chunk), F32),
             ((n_ep, rows, chunk), BF), ((n_tp, groups, group_slots, chunk), BF),
-            ((2, batch // 2, 2 * hidden), F32), ((2, batch // 2, 2 * hidden), BF),
-            ((batch // 2, 2 * hidden), BF), ((lines, batch // 2, 2 * hidden), BF),
-            ((2, batch // 2, hidden), BF),
+            ((steps, 2, unit_rows, 2 * hidden), F32), ((steps, 2, unit_rows, 2 * hidden), BF),
+            ((steps, unit_rows, 2 * hidden), BF), ((steps, lines, unit_rows, 2 * hidden), BF),
+            ((2 * steps, unit_rows, hidden), BF),
             ((2, groups, lines, group_slots, chunk), BF), ((groups, lines, group_slots, chunk), BF),
             ((groups, lines, group_slots, chunk), BF), ((groups, lines, group_slots, chunk), BF),
             ((groups, 2, members // 2, rows, chunk), F32),
             ((groups, members // 2, rows, chunk), BF), ((groups, members // 2, rows, chunk), BF),
-            ((pairs, rows, chunk), BF), ((pairs, rows, chunk), BF),
+            ((n_ep, rows, chunk), BF), ((n_ep, rows, chunk), BF),
             ((groups, members * rows, group_slots), BF), ((n_ep, rows, chunk), F32),
         )
     ]
@@ -608,7 +752,7 @@
         out_shape=(pltpu.HBM(delta_state.shape, F32), pltpu.HBM((rows, chunk), BF)),
         in_specs=[vmem] * 2,
         out_specs=(pl.BlockSpec(memory_space=pltpu.HBM),) * 2,
-        scratch_shapes=[pltpu.SemaphoreType.DMA((rows + 1,))],
+        scratch_shapes=[pltpu.SemaphoreType.DMA((2,))],
         compiler_params=pltpu.CompilerParams(vmem_limit_bytes=8 * 1024 * 1024),
     )(*(pltpu.with_memory_space_constraint(a, pltpu.VMEM) for a in (new_state, mixed_out)))
     return mixed_out, new_state

time: 64.4 us -> 60.2 us (0.935)
  Pallas kernels: 63.6 us -> 59.4 us
    pallas_call x1, Pallas kernels: 60.7 us -> 56.7 us  [per_device(): pl.pallas_call(functools.partial(kernel, dims), out_shape=(pltpu.VMEM((ro...]
where the time goes in v4:
time: 60.2 us; the launch traced here: 60 us
  Pallas kernels  59.4 us (99%)
  between operations  0.65 us (1%)
    pallas_call x1, Pallas kernels, per_device(): pl.pallas_call(functools.partial(kernel, dims), out_shape=(pltpu.VMEM((ro...  56.7 us
    pallas_call x1, Pallas kernels, per_device(): pl.pallas_call(store_kernel, out_shape=(pltpu.HBM(delta_state.shape, F32)...  2.66 us

profile of v4, /device:TPU:0, one launch (start us, length us, event | category | flops | bytes accessed | tf_op | source)
XLA Modules:
  0.0 60.0 jit_solution(7153589193574685125)
XLA Ops:
  0.6 56.7 %shard_map.221 = (bf16[24,1024]{1,0:T(8,128)(2,1)S(1)}, f32[24,4,128,128]{3,2,1,0:T(8,128)S(1)}) custom-call(bf16[24,4096]{1,0:T(8,128)(2,1)} %refs_0_.1, f32[1,4096]{1,0:T(1,128)} %bitcast.12, f32[1,4]{1,0:T(1,128)} %bitcast.17, f32[1,128]{1,0:T(1,128)} %bitcast.18, f32[1,4096]{1,0:T(1,128)} %bitcast.13, s32[2,24]{1,0:T(2,128)} %bitcast.15, ...), custom_call_target="tpu_custom_call" | custom-call | tf_op jit(solution)/shard_map/pallas_call | solution.py:740
  57.4 2.7 %shard_map.222 = (f32[24,4,128,128]{3,2,1,0:T(8,128)}, bf16[24,1024]{1,0:T(8,128)(2,1)}) custom-call(f32[24,4,128,128]{3,2,1,0:T(8,128)S(1)} %get-tuple-element.6.state, bf16[24,1024]{1,0:T(8,128)(2,1)S(1)} %get-tuple-element.7.mixed), custom_call_target="tpu_custom_call" | custom-call | tf_op jit(solution)/shard_map/pallas_call | solution.py:750

commit v5 on v4

--- a/solution.py
+++ b/solution.py
@@ -9,7 +9,11 @@
 from jax.sharding import PartitionSpec as P
 
 EPS = 1e-06
-CROSS_AT = 2
+CROSS_AT = 6
+DOTS_AT = 1
+RETURNS = (0, 1, 2, 3)
+LAG = 2
+STORE = 1
 RECALL = 4
 UPDATE = 4
 X_STRAIGHT = (2,)
@@ -55,8 +59,10 @@
     rows = state.shape[0]
     small = pltpu.make_async_copy(mixed, mixed_out, sems.at[1])
     small.start()
-    for r in range(rows):
-        pltpu.make_async_copy(state.at[r], state_out.at[r], sems.at[0]).start()
+    step = math.gcd(rows, STORE)
+    for r in range(0, rows, step):
+        block = pl.ds(r, step)
+        pltpu.make_async_copy(state.at[block], state_out.at[block], sems.at[0]).start()
     pltpu.make_async_copy(state, state_out, sems.at[0]).wait()
     small.wait()
 
@@ -72,9 +78,9 @@
     sizes = {
         "load": n_in, "ns": 1, "nr": pairs + 1, "ms": 1, "mr": 1, "cs": 1, "cr": 1, "zs": 1, "zr": 1,
         "q1s": 1, "q1r": 2, "q2s": 1, "q2r": 2, "k1s": 1, "k1r": 1, "k2s": 1, "k2r": 1, "xs": 1, "xr": n_ep,
-        "f1s": 1, "f1r": groups, "f2s": 1, "f2r": n_ep, "as": 1, "ar": 1, "ss": 1, "sr": 1,
+        "f1s": 1, "f1r": groups, "f2s": 1, "f2r": 1, "as": 1, "ar": 1, "ss": 1, "sr": 1,
         "d1s": 1, "d1r": steps, "d2s": 1, "d2r": steps * lines, "hs": 1, "hr": steps,
-        "gs": 1, "gr": groups * n_tp, "e1s": 1, "e1r": groups, "e2s": 1, "e2r": groups,
+        "gs": 1, "gr": groups * n_tp, "e1s": 1, "e1r": groups * lines, "e2s": 1, "e2r": groups,
     }
     starts, total = {}, 0
     for name, size in sizes.items():
@@ -512,14 +518,18 @@
         send_g(k, g)
         if k > 1:
             pass_on(k - 2, group_from[k - 2])
-        if steps == 2 and k == 1:
+        if steps == 2 and k == DOTS_AT:
             dense_dots(0)
     drains.append(ep_copy(x_all.at[most], x_all.at[most], "x", mate))
     drains.append(tp_copy(g_all.at[most_tp], g_all.at[most_tp], "g", sibling))
     for i in (eg_i, eu_i, ed_i, dd_i):
         loads[i].wait()
+    if steps == 2 and CROSS_AT == 6:
+        dense_cross(0)
     for h in range(0 if steps != 2 else 1, steps):
         dense_dots(h)
+    if steps == 2 and CROSS_AT == 7:
+        dense_cross(0)
     if groups > 1:
         pass_on(groups - 2, group_from[groups - 2])
     if steps == 2 and CROSS_AT == 4:
@@ -537,6 +547,8 @@
     for k in range(groups):
         arrived_g(k, group_from[k], sibling)
     gate, up = expert_in(sibling, gate, up)
+    if steps == 2 and CROSS_AT == 5:
+        dense_cross(0)
     for h in range(0 if steps != 2 else 1, steps):
         dense_cross(h)
     done_z = ep_copy(scale_rows.at[most], scale_rows.at[most], "z", mate)
@@ -565,11 +577,14 @@
             arrived_g(k, group_from[k], other_core(y))
         gate, up = expert_in(other_core(y), gate, up)
     expert_hidden = (silu(gate * slot_scale) * (up * slot_scale)).astype(BF)
-    returns = far_groups + [my_group]
-
-    def near_e(k):
+    order_back = RETURNS if groups == 4 else tuple(range(groups))
+    returns = [(far_groups + [my_group])[i] for i in order_back]
+    own_at = order_back.index(groups - 1)
+    f_direct = [k for k in range(groups) if order_back[k] in f_straight]
+
+    def near_e(k, y):
         g = returns[k]
-        return tp_copy(e_part.at[1 - core, g], e_near.at[g], "e1", sibling, k)
+        return tp_copy(e_part.at[1 - core, g, y], e_near.at[g, y], "e1", sibling, k * lines + y)
 
     def far_e(k, y):
         g = returns[k]
@@ -579,16 +594,16 @@
         part = dot(expert_hidden, w_ed[0, :, columns_of(2 * y + which)])
         e_part[which, :, y] = part.reshape(groups, group_slots, chunk).astype(BF)
 
-    for y in range(lines):
+    for y in far_lines + [line]:
         expert_out(1 - core, y)
-    for k in range(groups):
-        near_e(k).start()
-    for y in range(lines):
+        for k in range(groups):
+            near_e(k, y).start()
+    for y in far_lines + [line]:
         expert_out(core, y)
     for k in range(groups):
         g = returns[k]
-        near_e(k).wait_recv()
         for y in far_lines:
+            near_e(k, y).wait_recv()
             e_send[g, y] = (e_part[core, g, y].astype(F32) + e_near[g, y].astype(F32)).astype(BF)
             far_e(k, y).start()
     drains.append(tp_copy(e_part.at[0], e_near, "e1", sibling))
@@ -619,25 +634,26 @@
         near_f(k).wait_recv()
         both = comb[g, par] + f_mate[g].astype(F32)
         comb[g, par] = both
-        send_f(g, both, k == groups - 1)
+        send_f(g, both, k == own_at)
 
     def send_f(g, values, own_group):
         f_send[pl.ds(g * group_pairs, group_pairs)] = values.astype(BF)
         for q in pairs_in(g, own_group):
-            ep_copy(f_send.at[q], f_recv.at[pair], "f2", twin(q), pair).start()
+            ep_copy(f_send.at[q], f_recv.at[pair], "f2", twin(q)).start()
 
     def straight_f(k, g):
         send_f(g, comb[g, par], False)
-        first = pairs + f_straight.index(k) * group_pairs
+        first = pairs + f_straight.index(order_back[k]) * group_pairs
         f_send[pl.ds(first, group_pairs)] = comb[g, 1 - par].astype(BF)
         for m in range(group_pairs):
             spare = first + lax.rem(pair, group_pairs)
             q = g * group_pairs + m
-            ep_copy(f_send.at[first + m], f_recv.at[spare], "f2", cross(q), spare).start()
+            ep_copy(f_send.at[first + m], f_recv.at[spare], "f2", cross(q)).start()
 
     for k in range(groups):
         g = returns[k]
         block = pl.ds(g * members, members)
+        near_e(k, line).wait_recv()
         result = e_part[core, g, line].astype(F32) + e_near[g, line].astype(F32)
         tp_copy(e_send.at[g, other_lines], e_recv.at[g, other_lines], "e2", sibling, k).wait_recv()
         for y in far_lines:
@@ -647,24 +663,24 @@
         combined = dense_ref[block] + mixed.reshape(members, rows, chunk)
         for m in range(members):
             comb[g, m % 2, m // 2] = combined[m]
-        if k in f_straight:
+        if k in f_direct:
             straight_f(k, g)
         else:
             f_away[g] = comb[g, 1 - par].astype(BF)
             near_f(k).start()
-        if k > 1 and k - 2 not in f_straight:
-            far_f(k - 2)
-    for k in range(max(0, groups - 2), groups):
-        if k not in f_straight:
+        if k >= LAG and k - LAG not in f_direct:
+            far_f(k - LAG)
+    for k in range(max(0, groups - LAG), groups):
+        if k not in f_direct:
             far_f(k)
-    met = pl.ds(0, groups - len(f_straight))
+    met = pl.ds(0, groups - len(f_direct))
     drains.append(ep_copy(f_away.at[met], f_mate.at[met], "f1", mate))
     spares = list(range(pairs, pairs + len(f_straight) * group_pairs))
     sent = pl.ds(0, pairs - 1 + len(spares))
     drains.append(ep_copy(f_send.at[sent], f_recv.at[sent], "f2", mate))
     final = middle_ref[...] + comb[my_group, par, lax.rem(pair, group_pairs)]
+    ep_copy(f_send.at[sent], f_recv.at[sent], "f2", mate).wait_recv()
     for q in others + spares:
-        ep_copy(f_send.at[q], f_recv.at[q], "f2", mate, q).wait_recv()
         final = final + f_recv[q].astype(F32)
     out[...] = final.astype(BF)
     for copy in drains:

time: 60.2 us -> 59.1 us (0.982)
  Pallas kernels: 59.4 us -> 58.3 us
    pallas_call x1, Pallas kernels: 56.7 us -> 55.6 us  [per_device(): pl.pallas_call(functools.partial(kernel, dims), out_shape=(pltpu.VMEM((ro...]
where the time goes in v5:
time: 59.1 us; the launch traced here: 58.9 us
  Pallas kernels  58.3 us (99%)
  between operations  0.65 us (1%)
    pallas_call x1, Pallas kernels, per_device(): pl.pallas_call(functools.partial(kernel, dims), out_shape=(pltpu.VMEM((ro...  55.6 us
    pallas_call x1, Pallas kernels, per_device(): pl.pallas_call(store_kernel, out_shape=(pltpu.HBM(delta_state.shape, F32)...  2.66 us

profile of v5, /device:TPU:0, one launch (start us, length us, event | category | flops | bytes accessed | tf_op | source)
XLA Modules:
  0.0 58.9 jit_solution(5439944139893501817)
XLA Ops:
  0.6 55.6 %shard_map.221 = (bf16[24,1024]{1,0:T(8,128)(2,1)S(1)}, f32[24,4,128,128]{3,2,1,0:T(8,128)S(1)}) custom-call(bf16[24,4096]{1,0:T(8,128)(2,1)} %refs_0_.1, f32[1,4096]{1,0:T(1,128)} %bitcast.12, f32[1,4]{1,0:T(1,128)} %bitcast.17, f32[1,128]{1,0:T(1,128)} %bitcast.18, f32[1,4096]{1,0:T(1,128)} %bitcast.13, s32[2,24]{1,0:T(2,128)} %bitcast.15, ...), custom_call_target="tpu_custom_call" | custom-call | tf_op jit(solution)/shard_map/pallas_call | solution.py:756
  56.3 2.7 %shard_map.222 = (f32[24,4,128,128]{3,2,1,0:T(8,128)}, bf16[24,1024]{1,0:T(8,128)(2,1)}) custom-call(f32[24,4,128,128]{3,2,1,0:T(8,128)S(1)} %get-tuple-element.6.state, bf16[24,1024]{1,0:T(8,128)(2,1)S(1)} %get-tuple-element.7.mixed), custom_call_target="tpu_custom_call" | custom-call | tf_op jit(solution)/shard_map/pallas_call | solution.py:766

commit v6 on v5

--- a/solution.py
+++ b/solution.py
@@ -9,8 +9,6 @@
 from jax.sharding import PartitionSpec as P
 
 EPS = 1e-06
-CROSS_AT = 6
-DOTS_AT = 1
 RETURNS = (0, 1, 2, 3)
 LAG = 2
 STORE = 1
@@ -503,8 +501,6 @@
         g = group_from[k]
         if k < len(relayed):
             forward_x(relayed[k])
-        if steps == 2 and k == CROSS_AT:
-            dense_cross(0)
         if k > 0 and k not in relayed:
             for q in pairs_in(g):
                 ep_copy(x_all.at[me], x_all.at[twin(q)], "x", mate, twin(q)).wait_recv()
@@ -518,22 +514,18 @@
         send_g(k, g)
         if k > 1:
             pass_on(k - 2, group_from[k - 2])
-        if steps == 2 and k == DOTS_AT:
+        if steps == 2 and k == 1:
             dense_dots(0)
     drains.append(ep_copy(x_all.at[most], x_all.at[most], "x", mate))
     drains.append(tp_copy(g_all.at[most_tp], g_all.at[most_tp], "g", sibling))
     for i in (eg_i, eu_i, ed_i, dd_i):
         loads[i].wait()
-    if steps == 2 and CROSS_AT == 6:
+    if steps == 2:
         dense_cross(0)
     for h in range(0 if steps != 2 else 1, steps):
         dense_dots(h)
-    if steps == 2 and CROSS_AT == 7:
-        dense_cross(0)
     if groups > 1:
         pass_on(groups - 2, group_from[groups - 2])
-    if steps == 2 and CROSS_AT == 4:
-        dense_cross(0)
 
     def expert_in(p, gate, up):
         routed = g_all[p].astype(F32).reshape(slots, chunk).astype(BF)
@@ -544,13 +536,11 @@
     gate = jnp.zeros((slots, w_eg.shape[2]), F32)
     gate, up = expert_in(my, gate, gate)
     pass_on(groups - 1, group_from[groups - 1])
+    for h in range(0 if steps != 2 else 1, steps):
+        dense_cross(h)
     for k in range(groups):
         arrived_g(k, group_from[k], sibling)
     gate, up = expert_in(sibling, gate, up)
-    if steps == 2 and CROSS_AT == 5:
-        dense_cross(0)
-    for h in range(0 if steps != 2 else 1, steps):
-        dense_cross(h)
     done_z = ep_copy(scale_rows.at[most], scale_rows.at[most], "z", mate)
     done_z.wait_recv()
     drains.append(done_z)

time: 59.1 us -> 59.1 us (level)
  no operation moved by 1% of the time
where the time goes in v6:
time: 59.1 us; the launch traced here: 58.9 us
  Pallas kernels  58.3 us (99%)
  between operations  0.65 us (1%)
    pallas_call x1, Pallas kernels, per_device(): pl.pallas_call(functools.partial(kernel, dims), out_shape=(pltpu.VMEM((ro...  55.6 us
    pallas_call x1, Pallas kernels, per_device(): pl.pallas_call(store_kernel, out_shape=(pltpu.HBM(delta_state.shape, F32)...  2.66 us

profile of v6, /device:TPU:0, one launch (start us, length us, event | category | flops | bytes accessed | tf_op | source)
XLA Modules:
  0.0 58.9 jit_solution(15055327733285559451)
XLA Ops:
  0.6 55.6 %shard_map.221 = (bf16[24,1024]{1,0:T(8,128)(2,1)S(1)}, f32[24,4,128,128]{3,2,1,0:T(8,128)S(1)}) custom-call(bf16[24,4096]{1,0:T(8,128)(2,1)} %refs_0_.1, f32[1,4096]{1,0:T(1,128)} %bitcast.12, f32[1,4]{1,0:T(1,128)} %bitcast.17, f32[1,128]{1,0:T(1,128)} %bitcast.18, f32[1,4096]{1,0:T(1,128)} %bitcast.13, s32[2,24]{1,0:T(2,128)} %bitcast.15, ...), custom_call_target="tpu_custom_call" | custom-call | tf_op jit(solution)/shard_map/pallas_call | solution.py:746
  56.3 2.7 %shard_map.222 = (f32[24,4,128,128]{3,2,1,0:T(8,128)}, bf16[24,1024]{1,0:T(8,128)(2,1)}) custom-call(f32[24,4,128,128]{3,2,1,0:T(8,128)S(1)} %get-tuple-element.6.state, bf16[24,1024]{1,0:T(8,128)(2,1)S(1)} %get-tuple-element.7.mixed), custom_call_target="tpu_custom_call" | custom-call | tf_op jit(solution)/shard_map/pallas_call | solution.py:756

commit v7 on v6

--- a/solution.py
+++ b/solution.py
@@ -14,6 +14,7 @@
 STORE = 1
 RECALL = 4
 UPDATE = 4
+LOADED_WITH = (0,) * 9 + (1, 2, 2, 3, 3, 3, 4, 5, 5, 6, 6, 6, 6)
 X_STRAIGHT = (2,)
 F_STRAIGHT = (0, 2)
 X_SENDS = (0, 1, 2)
@@ -74,7 +75,7 @@
     pairs, lines = n_ep // 2, n_tp // 2
     steps = dense_steps(groups)
     sizes = {
-        "load": n_in, "ns": 1, "nr": pairs + 1, "ms": 1, "mr": 1, "cs": 1, "cr": 1, "zs": 1, "zr": 1,
+        "load": max(LOADED_WITH) + 1, "ns": 1, "nr": pairs + 1, "ms": 1, "mr": 1, "cs": 1, "cr": 1, "zs": 1, "zr": 1,
         "q1s": 1, "q1r": 2, "q2s": 1, "q2r": 2, "k1s": 1, "k1r": 1, "k2s": 1, "k2r": 1, "xs": 1, "xr": n_ep,
         "f1s": 1, "f1r": groups, "f2s": 1, "f2r": 1, "as": 1, "ar": 1, "ss": 1, "sr": 1,
         "d1s": 1, "d1r": steps, "d2s": 1, "d2r": steps * lines, "hs": 1, "hr": steps,
@@ -170,7 +171,7 @@
     drains = []
 
     loads = [
-        pltpu.make_async_copy(src, dst, sem("load", i))
+        pltpu.make_async_copy(src, dst, sem("load", LOADED_WITH[i]))
         for i, (src, dst) in enumerate(zip(hbm, held))
     ]
     state_i, decay_i, beta_i, q_i, k_i, v_i, o_i, dg_i, du_i, eg_i, eu_i, ed_i, dd_i = range(9, 22)

time: 59.1 us -> 58.9 us (level)
  no operation moved by 1% of the time
where the time goes in v7:
time: 58.9 us; the launch traced here: 58.8 us
  Pallas kernels  58.1 us (99%)
  between operations  0.65 us (1%)
    pallas_call x1, Pallas kernels, per_device(): pl.pallas_call(functools.partial(kernel, dims), out_shape=(pltpu.VMEM((ro...  55.5 us
    pallas_call x1, Pallas kernels, per_device(): pl.pallas_call(store_kernel, out_shape=(pltpu.HBM(delta_state.shape, F32)...  2.66 us

profile of v7, /device:TPU:0, one launch (start us, length us, event | category | flops | bytes accessed | tf_op | source)
XLA Modules:
  0.0 58.8 jit_solution(7474161146374788127)
XLA Ops:
  0.6 55.5 %shard_map.221 = (bf16[24,1024]{1,0:T(8,128)(2,1)S(1)}, f32[24,4,128,128]{3,2,1,0:T(8,128)S(1)}) custom-call(bf16[24,4096]{1,0:T(8,128)(2,1)} %refs_0_.1, f32[1,4096]{1,0:T(1,128)} %bitcast.12, f32[1,4]{1,0:T(1,128)} %bitcast.17, f32[1,128]{1,0:T(1,128)} %bitcast.18, f32[1,4096]{1,0:T(1,128)} %bitcast.13, s32[2,24]{1,0:T(2,128)} %bitcast.15, ...), custom_call_target="tpu_custom_call" | custom-call | tf_op jit(solution)/shard_map/pallas_call | solution.py:747
  56.1 2.7 %shard_map.222 = (f32[24,4,128,128]{3,2,1,0:T(8,128)}, bf16[24,1024]{1,0:T(8,128)(2,1)}) custom-call(f32[24,4,128,128]{3,2,1,0:T(8,128)S(1)} %get-tuple-element.6.state, bf16[24,1024]{1,0:T(8,128)(2,1)S(1)} %get-tuple-element.7.mixed), custom_call_target="tpu_custom_call" | custom-call | tf_op jit(solution)/shard_map/pallas_call | solution.py:757
